TPU v7x, 256 devices: a whole 4x4x8 slice. The times are simulated.
256 devices in a mesh: sp: 64 (over z, x, core), tp: 4 (over y).
Axes of the slice: x: 4, y: 4, z: 8, core: 2. Of those that a mesh axis runs over, the one named last changes fastest.
Arguments:
- stream: bfloat16 [8192, 2048], P(('sp', 'tp')), may hold values from -2.5 to 2.5
- recurrence_input: bfloat16 [8192, 2, 1024], P('sp', None, 'tp'), may hold values from -6 to 6
- output_gate_input: bfloat16 [8192, 2, 1024], P('sp', None, 'tp'), may hold values from -6 to 6
- convolution_taps: bfloat16 [4, 2, 1024], P(None, None, 'tp'), may hold values from -4 to 4
- first_group_gates: bfloat16 [2, 16, 64, 64], P(None, 'tp'), may hold values from -0.75 to 0.75
- second_group_gates: bfloat16 [2, 8, 128, 128], P(None, 'tp'), may hold values from -0.5 to 0.5
- channel_decay: float32 [2, 1024], P(None, 'tp'), may hold values from 4.7 to 13.6
- position_log_extra: float32 [8192, 2, 1024], P('sp', None, 'tp'), may hold values from -1.4 to 0, as said below
- recurrence_output_weight: bfloat16 [2, 1024, 2048], P(None, 'tp'), may hold values from -0.125 to 0.125
- first_norm_gain: float32 [2048], replicated, may hold values from 0.1 to 1.9
- first_norm_bias: float32 [2048], replicated, may hold values from -1.75 to 1.75
- routed_expert_index: int32 [8192, 4], P('sp'), may hold values from 0 to 63, all different within a row; in each aligned block of 32 rows (0 to 31, 32 to 63, ...) at most 2 rows name the same one
- routed_expert_weight: float32 [8192, 4], P('sp'), may hold values from 0.25 to 1
- routed_gate_weight: bfloat16 [64, 2048, 512], P('sp', None, 'tp'), may hold values from -0.125 to 0.125
- routed_up_weight: bfloat16 [64, 2048, 512], P('sp', None, 'tp'), may hold values from -0.125 to 0.125
- routed_down_weight: bfloat16 [64, 512, 2048], P('sp', 'tp'), may hold values from -0.25 to 0.25
- shared_gate_weight: bfloat16 [2048, 512], replicated, may hold values from -0.125 to 0.125
- shared_up_weight: bfloat16 [2048, 512], replicated, may hold values from -0.125 to 0.125
- shared_down_weight: bfloat16 [512, 2048], replicated, may hold values from -0.25 to 0.25
- second_norm_gain: float32 [2048], replicated, may hold values from 0.1 to 1.9
- second_norm_bias: float32 [2048], replicated, may hold values from -1.75 to 1.75
Outputs:
- result: bfloat16 [8192, 2048], P(('sp', 'tp'))
Inputs may be any that keep to these rules, and one draw needn't show every extreme that they name: `routed_expert_index`: each row names 4 different experts. In each aligned block of 32 rows no expert is named more than 2 times, and in some block an expert is named exactly 2 times. `position_log_extra`: every entry is negative.
All inputs are finite; a program needn't handle non-finite values.
Results may differ from a plain program's by a relative error of at most 0.015.
Values may be sent and summed in bfloat16 or wider, within the bound.
A program may use at most 64 MiB of HBM per device.

v0:
```python
import jax
import jax.numpy as jnp
from jax import lax
from jax.sharding import PartitionSpec as P

RESIDUAL_SCALE = 8.0**0.25
NORM_EPSILON = 1e-05


def copy_for_each(shard, axis):
    count = lax.axis_size(axis)
    return lax.all_to_all(
        jnp.broadcast_to(shard[None], (count, *shard.shape)), axis, 0, 0, tiled=True
    )


def all_in_one(shard, axis):
    leaves = jax.tree.leaves(shard)
    sequence = sorted(range(len(leaves)), key=lambda k: -leaves[k].size)
    width = (1, *leaves[sequence[0]].shape)[-1]
    lines = [
        jnp.pad(leaves[k].reshape(-1), (0, -leaves[k].size % width)).reshape(-1, width)
        for k in sequence
    ]
    both, at, found = (copy_for_each(jnp.concatenate(lines), axis), 0, {})
    for k, line in zip(sequence, lines):
        slab = both[:, at : at + len(line)].reshape(len(both), -1)
        found[k] = slab[:, : leaves[k].size].reshape(-1, *leaves[k].shape)
        at += len(line)
    numbers = iter(range(len(leaves)))
    return jax.tree.map(lambda _: found[next(numbers)], shard)


def joined_by_halves(pieces, combine):
    while len(jax.tree.leaves(pieces)[0]) > 1:
        pieces = jax.vmap(combine)(
            *(jax.tree.map(lambda part: part[side::2], pieces) for side in (0, 1))
        )
    return jax.tree.map(lambda part: part[0], pieces)


def entering(shard, axis, combine, identity):
    count, mine = (lax.axis_size(axis), lax.axis_index(axis))
    passed = jnp.arange(count) < mine

    def kept(part, zero, own):
        part = jnp.where(
            passed.reshape(-1, *(1 for _ in own.shape)), part, jnp.asarray(zero, own.dtype)
        )
        return part

    pieces = all_in_one(shard, axis)
    return joined_by_halves(jax.tree.map(kept, pieces, identity, shard), combine)


def shifted(shard, axis, by):
    count = lax.axis_size(axis)
    pairs = [(i, i + by) for i in range(count) if 0 <= i + by < count]
    return lax.ppermute(shard, axis, pairs)


def cut_along(shard, dim, count):
    dims = shard.shape
    pieces = shard.reshape(*dims[:dim], count, dims[dim] // count, *dims[dim + 1 :])
    return jnp.moveaxis(pieces, dim, 0)


def summed_on_arrival(shard, axis, dim):
    count = lax.axis_size(axis)
    pieces = lax.all_to_all(cut_along(shard, dim, count), axis, 0, 0, tiled=True)
    return jnp.sum(pieces.astype(jnp.float32), axis=0)


def layer_norm(values, gain_vec, bias_vec):
    row_mean = jnp.mean(values, axis=-1, keepdims=True)
    spread = jnp.mean(jnp.square(values - row_mean), axis=-1, keepdims=True)
    return (values - row_mean) * lax.rsqrt(spread + NORM_EPSILON) * gain_vec + bias_vec


def block_gates(conv_rows, weights, head_size):
    length = conv_rows.shape[0]
    head_rows = conv_rows.reshape(length, -1, head_size)
    pre_act = jnp.einsum("thc,ghcd->gthd", head_rows, weights, preferred_element_type=jnp.float32)
    gate_pair = jax.nn.sigmoid(pre_act).reshape(2, length, -1)
    return (gate_pair[0], gate_pair[1])


def chain_link(first_part, second_part):
    return (first_part[0] * second_part[0], second_part[0] * first_part[1] + second_part[1])


def carried(totals):
    unity = jnp.ones_like(totals[0])
    nought = jnp.zeros_like(totals[1])
    return entering(totals, "sp", chain_link, (unity, nought))[1]


def expert_terms(picked, letters, gate_w, up_w, down_w):
    gate_form = letters + "d,ldf->" + letters + "f"
    down_form = letters + "f,lfd->" + letters + "d"
    gated = jnp.einsum(gate_form, picked, gate_w, preferred_element_type=jnp.float32)
    lifted = jnp.einsum(gate_form, picked, up_w, preferred_element_type=jnp.float32)
    hidden = (jax.nn.silu(gated) * lifted).astype(jnp.bfloat16)
    return jnp.einsum(down_form, hidden, down_w, preferred_element_type=jnp.float32)


def shards(
    stream,
    recurrence_input,
    output_gate_input,
    convolution_taps,
    first_group_gates,
    second_group_gates,
    channel_decay,
    position_log_extra,
    recurrence_output_weight,
    first_norm_gain,
    first_norm_bias,
    routed_expert_index,
    routed_expert_weight,
    routed_gate_weight,
    routed_up_weight,
    routed_down_weight,
    shared_gate_weight,
    shared_up_weight,
    shared_down_weight,
    second_norm_gain,
    second_norm_bias,
):
    length = recurrence_input.shape[0]
    tap_count = convolution_taps.shape[0]
    border = shifted(recurrence_input[length - (tap_count - 1) :], "sp", 1)
    padded = jnp.concatenate([border, recurrence_input], axis=0).astype(jnp.float32)
    tap_weights = convolution_taps.astype(jnp.float32)
    summed = tap_weights[0] * padded[0:length]
    for offset in range(1, tap_count):
        summed = summed + tap_weights[offset] * padded[offset : offset + length]
    conv_rows = summed.astype(jnp.bfloat16)
    recur_a, input_a = block_gates(conv_rows[:, 0], first_group_gates, first_group_gates.shape[-1])
    recur_b, input_b = block_gates(
        conv_rows[:, 1], second_group_gates, second_group_gates.shape[-1]
    )
    recurrence_gate = jnp.stack([recur_a, recur_b], axis=1)
    input_gate = jnp.stack([input_a, input_b], axis=1)
    decay_logarithm = -8.0 * recurrence_gate * jax.nn.softplus(-channel_decay) + position_log_extra
    decay_rate = jnp.exp(decay_logarithm)
    driving = (
        jnp.sqrt(-jnp.expm1(2.0 * decay_logarithm)) * input_gate * conv_rows.astype(jnp.float32)
    )
    running = jnp.cumsum(decay_logarithm, axis=0)
    tail_sum = jnp.sum(jnp.exp(running[-1] - running) * driving, axis=0)
    incoming = carried((jnp.exp(running[-1]), tail_sum))
    opening = driving[:1] + decay_rate[:1] * incoming
    started = jnp.concatenate([opening, driving[1:]], axis=0)
    states = lax.associative_scan(chain_link, (decay_rate, started), axis=0)[1]
    branch_output = (jax.nn.gelu(output_gate_input.astype(jnp.float32)) * states).astype(
        jnp.bfloat16
    )
    tp_count = lax.axis_size("tp")
    quarter = length // tp_count
    mixed = summed_on_arrival(
        jnp.einsum(
            "tgc,gcd->td",
            branch_output,
            recurrence_output_weight,
            preferred_element_type=jnp.float32,
        ).astype(jnp.bfloat16),
        "tp",
        0,
    )
    normed = layer_norm(
        RESIDUAL_SCALE * stream.astype(jnp.float32) + mixed, first_norm_gain, first_norm_bias
    ).astype(jnp.bfloat16)
    width = normed.shape[1]
    top_count = routed_expert_index.shape[1]
    local_count = routed_gate_weight.shape[0]
    expert_count = local_count * lax.axis_size("sp")
    capacity = max(2, 5 * quarter * top_count // (4 * expert_count))
    block_ids = routed_expert_index.reshape(tp_count, quarter * top_count)
    onehot = (
        block_ids[:, :, None] == jnp.arange(expert_count, dtype=jnp.int32)[None, None, :]
    ).astype(jnp.int32)
    slot_ranks = jnp.sum((jnp.cumsum(onehot, axis=1) - onehot) * onehot, axis=2)
    own_index = lax.axis_index("tp")
    own_ids = lax.dynamic_index_in_dim(block_ids, own_index, 0, keepdims=False)
    own_ranks = lax.dynamic_index_in_dim(slot_ranks, own_index, 0, keepdims=False)
    blank_row = jnp.zeros((1, width), jnp.bfloat16)
    padded_rows = jnp.concatenate([normed, blank_row], axis=0)
    targets = own_ids * capacity + own_ranks
    sources = jnp.arange(quarter * top_count, dtype=jnp.int32) // top_count
    table = jnp.full((expert_count * capacity,), quarter, jnp.int32).at[targets].set(sources)
    outgoing = jnp.take(padded_rows, table, axis=0).reshape(expert_count, capacity, width)
    arrived = lax.all_to_all(outgoing, "sp", split_axis=0, concat_axis=0, tiled=True)
    slots = arrived.shape[1]
    fanned = lax.all_gather(arrived[None], "tp", axis=0, tiled=True)
    shaped = fanned.reshape(tp_count, -1, local_count, slots, width)
    partial_value = expert_terms(
        shaped, "xslc", routed_gate_weight, routed_up_weight, routed_down_weight
    )
    summed_rows = summed_on_arrival(partial_value.astype(jnp.bfloat16), "tp", 0)
    leaving = summed_rows.astype(jnp.bfloat16).reshape(-1, slots, width)
    returned = lax.all_to_all(leaving, "sp", split_axis=0, concat_axis=0, tiled=True)
    picked_rows = returned.reshape(expert_count * capacity, width)[own_ids * capacity + own_ranks]
    own_weights = lax.dynamic_slice_in_dim(routed_expert_weight, own_index * quarter, quarter, 0)
    routed = jnp.sum(
        own_weights[:, :, None]
        * picked_rows.reshape(quarter, top_count, width).astype(jnp.float32),
        axis=1,
    )
    shared_hidden = (
        jax.nn.silu(jnp.dot(normed, shared_gate_weight, preferred_element_type=jnp.float32))
        * jnp.dot(normed, shared_up_weight, preferred_element_type=jnp.float32)
    ).astype(jnp.bfloat16)
    shared_out = jnp.dot(shared_hidden, shared_down_weight, preferred_element_type=jnp.float32)
    final = layer_norm(
        RESIDUAL_SCALE * normed.astype(jnp.float32) + (shared_out + routed),
        second_norm_gain,
        second_norm_bias,
    )
    return final.astype(jnp.bfloat16)


def solution(mesh):
    in_specs = (
        P(("sp", "tp"), None),
        P("sp", None, "tp"),
        P("sp", None, "tp"),
        P(None, None, "tp"),
        P(None, "tp", None, None),
        P(None, "tp", None, None),
        P(None, "tp"),
        P("sp", None, "tp"),
        P(None, "tp", None),
        P(),
        P(),
        P("sp", None),
        P("sp", None),
        P("sp", None, "tp"),
        P("sp", None, "tp"),
        P("sp", "tp", None),
        P(),
        P(),
        P(),
        P(),
        P(),
    )
    out_specs = P(("sp", "tp"), None)
    return jax.shard_map(shards, mesh=mesh, in_specs=in_specs, out_specs=out_specs, check_vma=False)
```

profile of v0, /device:TPU:1, one launch (start us, length us, event | category | flops | bytes accessed | tf_op | source)
XLA Modules:
  0.0 205.7 jit_solution(793034132163294517)
XLA Ops:
  6.5 1.1 copy.130
  7.6 4.5 %collective-permute-start = (bf16[3,2,256]{2,0,1:T(4,128)(2,1)S(1)}, bf16[3,2,256]{2,0,1:T(4,128)(2,1)S(1)}, u32[]{:S(2)}, u32[]{:S(2)}) collective-permute-start(bf16[3,2,256]{2,0,1:T(4,128)(2,1)S(1)} %slice.395), channel_id=1, source_target_pairs={{0,4},{4,8},{8,12},{12,16},{16,20},{20,24},{24,28},{28,32},{32,36}... | collective-permute-start | bytes 9224 | tf_op jit(solution)/shard_map/ppermute | solution.py:59
  12.1 0.7 convert_element_type.67
  12.9 0.7 fusion.84
  13.6 0.8 copy.147
  14.4 0.7 reshape.136
  15.1 0.1 fusion.45
  15.2 0.1 copy.132
  15.4 0.3 fusion.20
  15.7 0.1 copy.138
  15.8 0.1 copy.134
  16.0 0.3 fusion.16
  16.3 0.1 copy.165
  16.4 1.0 fusion.101
  17.4 0.2 fusion.53
  17.6 0.6 slice_bitcast_fusion
  18.1 0.6 fusion.99
  18.7 0.1 copy.141
  18.8 0.8 copy.166
  19.6 1.2 fusion.52
  20.9 0.7 broadcast_in_dim.61
  21.6 11.3 %all-to-all-start = ((f32[64,4,256]{2,1,0:T(4,128)}), f32[64,4,256]{2,1,0:T(4,128)S(1)}, u32[]{:S(2)}, u32[]{:S(2)}) async-start(f32[64,4,256]{2,1,0:T(4,128)} %broadcast_in_dim.61), calls=%async_computation | async-start | bytes 524288 | tf_op jit(solution)/shard_map/all_to_all | solution.py:12
  32.9 0.8 fusion.60
  33.7 0.3 reduce_window_sum.23
  34.0 0.9 select_reduce_fusion
  34.9 0.7 fusion.90
  35.6 1.5 scatter_custom_fusion
  37.1 0.7 slice.345
  37.9 0.7 slice.343
  38.7 7.3 %all-to-all-done = f32[64,4,256]{2,1,0:T(4,128)S(1)} async-done(((f32[64,4,256]{2,1,0:T(4,128)}), f32[64,4,256]{2,1,0:T(4,128)S(1)}, u32[]{:S(2)}, u32[]{:S(2)}) %all-to-all-start) | async-done | bytes 262176 | tf_op jit(solution)/shard_map/all_to_all | solution.py:12
  46.0 0.1 fusion.103
  46.2 0.6 slice.315
  46.8 0.6 slice.316
  47.5 0.9 fusion.109
  49.0 1.0 fusion.106
  51.7 1.3 fusion.1
  53.0 4.3 %all-to-all-start.1 = ((bf16[4,32,2048]{2,1,0:T(8,128)(2,1)}), bf16[4,32,2048]{2,1,0:T(8,128)(2,1)S(1)}, u32[]{:S(2)}, u32[]{:S(2)}) async-start(bf16[4,32,2048]{2,1,0:T(8,128)(2,1)} %bitcast.17), calls=%async_computation.1 | async-start | bytes 1048576 | tf_op jit(solution)/shard_map/all_to_all | solution.py:70
  57.3 0.1 broadcast_in_dim.65
  57.5 8.8 %all-to-all-done.1 = bf16[4,32,2048]{2,1,0:T(8,128)(2,1)S(1)} async-done(((bf16[4,32,2048]{2,1,0:T(8,128)(2,1)}), bf16[4,32,2048]{2,1,0:T(8,128)(2,1)S(1)}, u32[]{:S(2)}, u32[]{:S(2)}) %all-to-all-start.1) | async-done | bytes 524320 | tf_op jit(solution)/shard_map/all_to_all | solution.py:70
  66.4 0.2 fusion.71
  66.6 0.2 multiply_reduce_fusion.2
  66.8 0.1 add_convert_fusion.1
  67.0 0.9 gather_fusion
  67.9 1.1 gather.10
  69.0 1.6 broadcast_select_fusion
  70.6 23.1 %all_to_all.25 = bf16[64,2,2048]{2,1,0:T(2,128)(2,1)S(1)} all-to-all(bf16[64,2,2048]{2,1,0:T(2,128)(2,1)S(1)} %broadcast_select_fusion), channel_id=1, replica_groups=mesh['sp'=64,'tp'=4] {'sp'}, dimensions={0} | all-to-all | bytes 1048576 | tf_op jit(solution)/shard_map/all_to_all | solution.py:193
  93.8 1.0 copy.148
  94.8 27.8 %all-gather.3.cloned.1.call-done = bf16[256,2,2048]{2,0,1:T(8,128)(2,1)} async-done(((bf16[64,2,2048]{2,0,1:T(8,128)(2,1)}), bf16[256,2,2048]{2,0,1:T(8,128)(2,1)}) %all-gather.3.cloned.1.call-update) | async-done | bytes 2097168 | tf_op jit(solution)/shard_map/all_gather | solution.py:195
  122.6 2.4 %fusion.7 = f32[4,64,1,2,128]{4,1,3,0,2:T(8,128)S(1)} fusion(bf16[4,64,2,2048]{3,1,0,2:T(8,128)(2,1)} %bitcast.118, bf16[1,2048,128]{2,1,0:T(8,128)(2,1)} %param.34), kind=kOutput, calls=%fused_computation.14 | convolution fusion | flops 268435456 | bytes 2883584 | tf_op jit(solution)/shard_map/xslcd,ldf->xslcf/dot_general | solution.py:101
  125.0 5.2 %fusion = bf16[4,1,64,1,2,2048]{5,2,4,3,1,0:T(8,128)(2,1)} fusion(bf16[4,64,2,2048]{3,1,0,2:T(8,128)(2,1)} %bitcast.119, bf16[1,128,2048]{2,1,0:T(8,128)(2,1)S(1)} %copy-done.2, bf16[1,2048,128]{2,1,0:T(8,128)(2,1)S(1)} %copy-done.3, f32[4,64,1,2,128]{4,1,3,0,2:T(8,128)S(1)} %fusion.7), kind=kOutput, calls=%fused_computation.4 | convolution fusion | flops 538312704 | bytes 5505024 | tf_op jit(solution)/shard_map/xslcf,lfd->xslcd/dot_general | solution.py:104
  130.2 28.9 %all_to_all.26 = bf16[4,1,64,1,2,2048]{5,2,4,3,1,0:T(8,128)(2,1)S(1)} all-to-all(bf16[4,1,64,1,2,2048]{5,2,4,3,1,0:T(8,128)(2,1)} %fusion), channel_id=1, replica_groups=mesh['sp'=64,'tp'=4] {'tp'}, dimensions={0} | all-to-all | bytes 4194304 | tf_op jit(solution)/shard_map/all_to_all | solution.py:70
  159.2 0.4 bitcast_reduce_fusion
  159.5 1.3 copy.153
  160.9 11.9 %all-to-all-start.4 = ((bf16[64,2,2048]{2,1,0:T(2,128)(2,1)}), bf16[64,2,2048]{2,1,0:T(2,128)(2,1)S(1)}, u32[]{:S(2)}, u32[]{:S(2)}) async-start(bf16[64,2,2048]{2,1,0:T(2,128)(2,1)} %copy.153), calls=%async_computation.4 | async-start | bytes 1048576 | tf_op jit(solution)/shard_map/all_to_all | solution.py:202
  172.9 0.1 copy.146
  173.0 2.7 %fusion.118 = f32[32,512]{1,0:T(8,128)} fusion(bf16[32,2048]{1,0:T(8,128)(2,1)S(1)} %add_convert_fusion.1, bf16[2048,512]{1,0:T(8,128)(2,1)} %param.37), kind=kOutput, calls=%fused_computation.192 | convolution fusion | flops 67108864 | bytes 2293760 | tf_op jit(solution)/shard_map/dot_general | solution.py:211
  175.6 14.8 %all-to-all-done.4 = bf16[64,2,2048]{2,1,0:T(2,128)(2,1)S(1)} async-done(((bf16[64,2,2048]{2,1,0:T(2,128)(2,1)}), bf16[64,2,2048]{2,1,0:T(2,128)(2,1)S(1)}, u32[]{:S(2)}, u32[]{:S(2)}) %all-to-all-start.4) | async-done | bytes 524320 | tf_op jit(solution)/shard_map/all_to_all | solution.py:202
  190.5 0.2 reshape.142
  190.7 1.7 gather_fusion.1
  192.4 1.4 reshape.143
  193.8 0.7 multiply_reduce_fusion
  194.5 3.3 %fusion.117 = (f32[32]{0:T(128)S(1)}, f32[32,2048]{1,0:T(8,128)S(1)}) fusion(f32[32,2048]{1,0:T(8,128)S(1)} %multiply_reduce_fusion, bf16[512,2048]{1,0:T(8,128)(2,1)} %param.39, bf16[32,2048]{1,0:T(8,128)(2,1)S(1)} %add_convert_fusion.1, bf16[2048,512]{1,0:T(8,128)(2,1)} %param.38, f32[32,512]{1,0:T(8,128)} %fusion.118), kind=kOutput, calls=%fused_computation.191 | convolution fusion | flops 134643680 | bytes 4915328 | tf_op jit(solution)/shard_map/dot_general | solution.py:214
  197.8 0.2 multiply_reduce_fusion.1
  198.0 0.8 add_convert_fusion
  (165 shorter events, 2.6 us)
Async XLA Ops:
  6.5 45.1 %copy-start = (bf16[2,256,2048]{2,1,0:T(8,128)(2,1)S(1)}, bf16[2,256,2048]{2,1,0:T(8,128)(2,1)}, u32[]{:S(2)}) copy-start(bf16[2,256,2048]{2,1,0:T(8,128)(2,1)} %param.29) | copy-start | bytes 6291460
  6.5 8.9 %copy-start.19 = (bf16[2,4,64,64]{3,2,1,0:T(8,128)(2,1)S(1)}, bf16[2,4,64,64]{3,2,1,0:T(8,128)(2,1)}, u32[]{:S(2)}) copy-start(bf16[2,4,64,64]{3,2,1,0:T(8,128)(2,1)} %param.25) | copy-start | bytes 196612
  7.6 7.4 %collective-permute-start = (bf16[3,2,256]{2,0,1:T(4,128)(2,1)S(1)}, bf16[3,2,256]{2,0,1:T(4,128)(2,1)S(1)}, u32[]{:S(2)}, u32[]{:S(2)}) collective-permute-start(bf16[3,2,256]{2,0,1:T(4,128)(2,1)S(1)} %slice.395), channel_id=1, source_target_pairs={{0,4},{4,8},{8,12},{12,16},{16,20},{20,24},{24,28},{28,32},{32,36}... | collective-permute-start | bytes 9224 | tf_op jit(solution)/shard_map/ppermute | solution.py:59
  12.8 2.5 %copy-start.7 = (f32[2,256]{1,0:T(2,128)}, f32[2,256]{1,0:T(2,128)S(1)}, u32[]{:S(2)}) copy-start(f32[2,256]{1,0:T(2,128)S(1)} %get-tuple-element.37) | copy-start | bytes 6148
  12.8 2.5 %copy-start.8 = (f32[2,256]{1,0:T(2,128)}, f32[2,256]{1,0:T(2,128)S(1)}, u32[]{:S(2)}) copy-start(f32[2,256]{1,0:T(2,128)S(1)} %get-tuple-element.38) | copy-start | bytes 6148
  12.8 2.5 %copy-start.9 = (f32[2,256]{1,0:T(2,128)}, f32[2,256]{1,0:T(2,128)S(1)}, u32[]{:S(2)}) copy-start(f32[2,256]{1,0:T(2,128)S(1)} %get-tuple-element.39) | copy-start | bytes 6148
  12.9 2.5 %copy-start.10 = (f32[2,256]{1,0:T(2,128)}, f32[2,256]{1,0:T(2,128)S(1)}, u32[]{:S(2)}) copy-start(f32[2,256]{1,0:T(2,128)S(1)} %get-tuple-element.40) | copy-start | bytes 6148
  15.0 0.9 copy-start.20
  19.6 1.2 copy-start.15
  21.6 24.4 %all-to-all-start = ((f32[64,4,256]{2,1,0:T(4,128)}), f32[64,4,256]{2,1,0:T(4,128)S(1)}, u32[]{:S(2)}, u32[]{:S(2)}) async-start(f32[64,4,256]{2,1,0:T(4,128)} %broadcast_in_dim.61), calls=%async_computation | async-start | bytes 524288 | tf_op jit(solution)/shard_map/all_to_all | solution.py:12
  35.6 12.9 %copy-start.17 = (s32[128]{0:T(128)}, s32[128]{0:T(128)S(1)}, u32[]{:S(2)}) copy-start(s32[128]{0:T(128)S(1)} %fusion.90) | copy-start | bytes 1540
  48.9 1.2 copy-start.5
  50.3 1.2 copy-start.6
  50.8 0.9 copy-start.4
  51.7 5.6 %copy-start.21 = (s32[128]{0:T(128)S(1)}, s32[128]{0:T(128)}, u32[]{:S(2)}) copy-start(s32[128]{0:T(128)} %scatter_custom_fusion) | copy-start | bytes 1540
  51.7 14.7 %copy-start.1 = (bf16[32,2048]{1,0:T(8,128)(2,1)S(1)}, bf16[32,2048]{1,0:T(8,128)(2,1)}, u32[]{:S(2)}) copy-start(bf16[32,2048]{1,0:T(8,128)(2,1)} %param.21) | copy-start | bytes 393220
  53.0 13.8 %copy-start.11 = (f32[2048]{0:T(1024)S(1)}, f32[2048]{0:T(1024)}, u32[]{:S(2)}) copy-start(f32[2048]{0:T(1024)} %param.31) | copy-start | bytes 24580
  53.0 13.8 %copy-start.12 = (f32[2048]{0:T(1024)S(1)}, f32[2048]{0:T(1024)}, u32[]{:S(2)}) copy-start(f32[2048]{0:T(1024)} %param.30) | copy-start | bytes 24580
  53.0 13.3 %all-to-all-start.1 = ((bf16[4,32,2048]{2,1,0:T(8,128)(2,1)}), bf16[4,32,2048]{2,1,0:T(8,128)(2,1)S(1)}, u32[]{:S(2)}, u32[]{:S(2)}) async-start(bf16[4,32,2048]{2,1,0:T(8,128)(2,1)} %bitcast.17), calls=%async_computation.1 | async-start | bytes 1048576 | tf_op jit(solution)/shard_map/all_to_all | solution.py:70
  57.3 65.3 %all-gather.3.cloned.1.call-start = ((), (), s32[]{:S(2)}) async-start(), calls=%async_computation.5 | async-start | bytes 2621440 | tf_op jit(solution)/shard_map/all_gather | solution.py:195
  94.7 30.2 %copy-start.2 = (bf16[1,128,2048]{2,1,0:T(8,128)(2,1)S(1)}, bf16[1,128,2048]{2,1,0:T(8,128)(2,1)}, u32[]{:S(2)}) copy-start(bf16[1,128,2048]{2,1,0:T(8,128)(2,1)} %param.36) | copy-start | bytes 1572868
  94.7 30.2 %copy-start.3 = (bf16[1,2048,128]{2,1,0:T(8,128)(2,1)S(1)}, bf16[1,2048,128]{2,1,0:T(8,128)(2,1)}, u32[]{:S(2)}) copy-start(bf16[1,2048,128]{2,1,0:T(8,128)(2,1)} %param.35) | copy-start | bytes 1572868
  159.2 13.6 %copy-start.16 = (f32[128,4]{0,1:T(4,128)S(1)}, f32[128,4]{0,1:T(4,128)}, u32[]{:S(2)}) copy-start(f32[128,4]{0,1:T(4,128)} %param.33) | copy-start | bytes 6148
  159.2 13.8 %copy-start.18 = (s32[128]{0:T(128)S(1)}, s32[128]{0:T(128)}, u32[]{:S(2)}) copy-start(s32[128]{0:T(128)} %copy-done.17) | copy-start | bytes 1540
  160.9 29.6 %all-to-all-start.4 = ((bf16[64,2,2048]{2,1,0:T(2,128)(2,1)}), bf16[64,2,2048]{2,1,0:T(2,128)(2,1)S(1)}, u32[]{:S(2)}, u32[]{:S(2)}) async-start(bf16[64,2,2048]{2,1,0:T(2,128)(2,1)} %copy.153), calls=%async_computation.4 | async-start | bytes 1048576 | tf_op jit(solution)/shard_map/all_to_all | solution.py:202
  194.5 3.5 %copy-start.13 = (f32[2048]{0:T(1024)S(1)}, f32[2048]{0:T(1024)}, u32[]{:S(2)}) copy-start(f32[2048]{0:T(1024)} %param.41) | copy-start | bytes 24580
  194.5 3.5 %copy-start.14 = (f32[2048]{0:T(1024)S(1)}, f32[2048]{0:T(1024)}, u32[]{:S(2)}) copy-start(f32[2048]{0:T(1024)} %param.40) | copy-start | bytes 24580
Sparse Core Ops, SparseCore 0:
  94.9 27.6 all-gather.2
where the time goes:
time: 207 us; the launch traced here: 206 us
  waiting for transfers between devices  58.8 us (28%)
  blocking collectives  52.1 us (25%)
  starting transfers between devices  32 us (15%)
  local copies, waits for them, and re-layouts  19.8 us (10%)
  matrix products  15.4 us (7%)
  between operations  14.3 us (7%)
  other arithmetic  13.3 us (6%)
    all_to_all x1, blocking collectives, summed_on_arrival(): lax.all_to_all(cut_along(shard, dim, count), axis, 0, 0, tiled=True)  28.9 us
    all_gather x1, waiting for transfers between devices, shards(): fanned = lax.all_gather(arrived[None], 'tp', axis=0, tiled=True)  27.8 us
    all_to_all x1, blocking collectives, shards(): lax.all_to_all(outgoing, 'sp', split_axis=0, concat_axis=0, tiled=True)  23.1 us
    all_to_all x1, waiting for transfers between devices, shards(): lax.all_to_all(leaving, 'sp', split_axis=0, concat_axis=0, tiled=True)  14.8 us
    all_to_all x1, starting transfers between devices, shards(): lax.all_to_all(leaving, 'sp', split_axis=0, concat_axis=0, tiled=True)  11.9 us
    all_to_all x1, starting transfers between devices, copy_for_each(): lax.all_to_all(jnp.broadcast_to(shard[None], (count, *shard.shape)), axis...  11.3 us
    all_to_all x1, waiting for transfers between devices, summed_on_arrival(): lax.all_to_all(cut_along(shard, dim, count), axis, 0, 0, tiled=True)  8.83 us
    all_to_all x1, waiting for transfers between devices, copy_for_each(): lax.all_to_all(jnp.broadcast_to(shard[None], (count, *shard.shape)), axis...  7.34 us
  transfers between devices with their start and end apart: 5, of which 4 were waited for; matrix products, arithmetic and copies ran while one was open for 6% of the time, Pallas kernels for 0%

commit v1 on v0

v1 whole, which is shorter than its diff:
```python
import jax
import jax.numpy as jnp
from jax import lax
from jax.experimental import pallas as pl
from jax.experimental.pallas import tpu as pltpu
from jax.sharding import PartitionSpec as P

RESIDUAL_SCALE = 8.0**0.25
NORM_EPSILON = 1e-05
MESH = pl.DeviceIdType.MESH
F32 = jnp.float32
BF16 = jnp.bfloat16

PLANE = 8
PLANES = 8
TPS = 4
HEAD_ROWS = 16
CHUNKS = 2
FAR_FIRST = (4, 3, 5, 2, 6, 1, 7)


def layer_norm(values, gain_vec, bias_vec):
    row_mean = jnp.mean(values, axis=-1, keepdims=True)
    centred = values - row_mean
    spread = jnp.mean(jnp.square(centred), axis=-1, keepdims=True)
    return centred * lax.rsqrt(spread + NORM_EPSILON) * gain_vec + bias_vec


def softplus_of_minus(d):
    u = jnp.exp(-jnp.abs(d))
    s = u / (2.0 + u)
    q = s * s
    series = jnp.full_like(s, 1.0 / 15.0)
    for odd in (13, 11, 9, 7, 5, 3, 1):
        series = series * q + 1.0 / odd
    return jnp.maximum(-d, 0.0) + 2.0 * s * series


def minus_expm1(z):
    series = jnp.full_like(z, 1.0 / 40320.0)
    for factor in (5040.0, 720.0, 120.0, 24.0, 6.0, 2.0, 1.0):
        series = series * z + 1.0 / factor
    return jnp.where(z > -0.25, -z * series, 1.0 - jnp.exp(z))


def dot(a, b):
    return jnp.dot(a, b, preferred_element_type=F32)


def mega(
    stream_h, rec_h, gatein_h, taps_h, small_gates_h, large_gates_h, decay_h, extra_h,
    wout_h, gain1_h, bias1_h, index_h, weight_h, gate_w_h, up_w_h, down_w_h,
    shared_gate_h, shared_up_h, shared_down_h, gain2_h, bias2_h,
    out_ref,
    stream, rec, gatein, taps, small_gates, large_gates, decay, extra,
    wout, gain1, bias1, index, weight, gate_w, up_w, down_w,
    shared_gate, shared_up, shared_down, gain2, bias2,
    rec_f, border, cum_p, cum_s, carry1, carry2, gelu_buf, branch,
    part, mixed_buf, normed, slot_buf, weight_buf,
    disp, arr1, disp2, arr2, moe_out, ret1, ret1p, ret2, acc,
    load_sem, own_sem, border_sem, weight_sem, carry_sem, mix_sem, disp_sem, ret_sem,
):
    sp = lax.axis_index("sp")
    tp = lax.axis_index("tp")
    zi = sp // PLANE
    pi = sp % PLANE
    sends = []

    def load(k, src, dst):
        copy = pltpu.make_async_copy(src, dst, load_sem.at[k])
        copy.start()
        return copy

    def remote(src, dst, sem, where, sp_to, tp_to):
        copy = pltpu.make_async_remote_copy(
            src_ref=src,
            dst_ref=dst,
            send_sem=sem.at[(0, *where)],
            recv_sem=sem.at[(1, *where)],
            device_id={"sp": sp_to, "tp": tp_to},
            device_id_type=MESH,
        )
        return copy

    def send(*args):
        copy = remote(*args)
        copy.start()
        sends.append(copy)

    def plane_peer(d):
        return zi * PLANE + (pi + d) % PLANE

    def z_peer(d):
        return ((zi + d) % PLANES) * PLANE + pi

    names = (
        (rec_h, rec), (small_gates_h, small_gates), (large_gates_h, large_gates), (taps_h, taps),
        (decay_h, decay), (extra_h, extra), (gatein_h, gatein), (gate_w_h, gate_w.at[tp]),
        (up_w_h, up_w.at[tp]), (down_w_h, down_w.at[tp]), (wout_h, wout), (index_h, index),
        (weight_h, weight), (stream_h, stream), (gain1_h, gain1), (bias1_h, bias1),
        (shared_gate_h, shared_gate), (shared_up_h, shared_up), (shared_down_h, shared_down),
        (gain2_h, gain2), (bias2_h, bias2),
    )
    loads = [load(k, src, dst) for k, (src, dst) in enumerate(names)]

    barrier = pltpu.get_barrier_semaphore()

    def greet(sp_to, tp_to):
        pl.semaphore_signal(
            barrier, inc=1, device_id={"sp": sp_to, "tp": tp_to}, device_id_type=MESH
        )

    for d in range(1, PLANE):
        greet(plane_peer(d), tp)
    for d in range(1, PLANES):
        greet(z_peer(d), tp)
    for d in range(1, TPS):
        greet(sp, (tp + d) % TPS)
    greet((sp + 63) % 64, tp)

    for k in range(6):
        loads[k].wait()
    length = rec.shape[0]
    rec_f[HEAD_ROWS:, :] = rec[...].astype(F32)
    row_i = lax.broadcasted_iota(jnp.int32, (64, 128), 0)
    col_i = lax.broadcasted_iota(jnp.int32, (64, 128), 1)
    put_low = (row_i == col_i).astype(BF16)
    put_high = (row_i + 64 == col_i).astype(BF16)
    blocks = []
    for which in range(2):
        maps = []
        for pair in range(2):
            low = dot(small_gates[which, 2 * pair], put_low)
            high = dot(small_gates[which, 2 * pair + 1], put_high)
            maps.append(jnp.concatenate([low, high], axis=0).astype(BF16))
        for head in range(2):
            maps.append(large_gates[which, head])
        blocks.append(maps)
    rate = -8.0 * softplus_of_minus(decay[...])
    tap_f = taps[...].astype(F32)

    def scanned(first, count):
        for b in range(4):
            lanes = slice(128 * b, 128 * b + 128)
            conv = tap_f[0:1, lanes] * rec_f[first + HEAD_ROWS - 3 : first + HEAD_ROWS - 3 + count, lanes]
            for k in range(1, 4):
                at = first + HEAD_ROWS - 3 + k
                conv = conv + tap_f[k : k + 1, lanes] * rec_f[at : at + count, lanes]
            conv = conv.astype(BF16)
            recur_gate = jax.nn.sigmoid(dot(conv, blocks[0][b]))
            input_gate = jax.nn.sigmoid(dot(conv, blocks[1][b]))
            log_decay = recur_gate * rate[:, lanes] + extra[first : first + count, lanes]
            p = jnp.exp(log_decay)
            s = jnp.sqrt(minus_expm1(2.0 * log_decay)) * input_gate * conv.astype(F32)
            p = p.reshape(count // 8, 8, 128)
            s = s.reshape(count // 8, 8, 128)
            row = lax.broadcasted_iota(jnp.int32, (count // 8, 8, 128), 1)
            for by in (1, 2, 4):
                p_prev = pltpu.roll(p, by, 1)
                s_prev = pltpu.roll(s, by, 1)
                s = jnp.where(row >= by, p * s_prev + s, s)
                p = jnp.where(row >= by, p * p_prev, p)
            p_in = jnp.ones((1, 128), F32)
            s_in = jnp.zeros((1, 128), F32)
            for t in range(count // 8):
                s_t = s[t] + p[t] * s_in
                p_t = p[t] * p_in
                cum_s[first + 8 * t : first + 8 * t + 8, lanes] = s_t
                cum_p[first + 8 * t : first + 8 * t + 8, lanes] = p_t
                s_in = s_t[7:8]
                p_in = p_t[7:8]

    scanned(HEAD_ROWS, length - HEAD_ROWS)

    pl.semaphore_wait(barrier, 7 + 7 + 3 + 1)
    send(rec.at[length - HEAD_ROWS :], border, border_sem, (), (sp + 1) % 64, tp)

    left = (tp + 3) % TPS
    right = (tp + 1) % TPS

    def weights_out(buf, slot, to, k):
        send(buf.at[slot], buf.at[slot], weight_sem, (k,), sp, to)

    def weights_in(buf, slot, k):
        remote(buf.at[slot], buf.at[slot], weight_sem, (k,), sp, left).wait_recv()

    opposite = (tp + 2) % TPS
    loads[7].wait()
    weights_out(gate_w, tp, left, 0)
    weights_out(gate_w, tp, right, 1)

    remote(rec.at[length - HEAD_ROWS :], border, border_sem, (), sp, tp).wait_recv()
    border_f = border[...].astype(F32)
    rec_f[0:HEAD_ROWS, :] = jnp.where(sp > 0, border_f, jnp.zeros_like(border_f))
    scanned(0, HEAD_ROWS)

    head_p = cum_p[HEAD_ROWS - 1 : HEAD_ROWS, :]
    head_s = cum_s[HEAD_ROWS - 1 : HEAD_ROWS, :]
    tail_p = cum_p[length - 1 : length, :]
    tail_s = cum_s[length - 1 : length, :]
    total_p = head_p * tail_p
    total_s = tail_p * head_s + tail_s
    mine1 = carry1.at[pi]
    for b in range(4):
        mine1[0, b : b + 1, :] = total_p[:, 128 * b : 128 * b + 128]
        mine1[1, b : b + 1, :] = total_s[:, 128 * b : 128 * b + 128]
    for d in FAR_FIRST:
        send(mine1, mine1, carry_sem, (0, d), plane_peer(d), tp)

    for k in (6, 11, 12):
        loads[k].wait()
    own_rows = pl.ds(pl.multiple_of(tp * 32, 32), 32)
    ids = index[own_rows, :]
    factors = weight[own_rows, :]
    slot = lax.broadcasted_iota(jnp.int32, (32, 128), 1)
    named = jnp.zeros((32, 128), F32)
    scaled = jnp.zeros((32, 128), F32)
    for k in range(4):
        hit = ids[:, k : k + 1] == slot // 2
        named = named + jnp.where(hit, 1.0, 0.0)
        scaled = scaled + jnp.where(hit, factors[:, k : k + 1], 0.0)
    below = lax.broadcasted_iota(jnp.int32, (32, 32), 0) > lax.broadcasted_iota(
        jnp.int32, (32, 32), 1
    )
    earlier = dot(below.astype(BF16), named.astype(BF16))
    right_slot = jnp.abs(earlier - (slot % 2).astype(F32)) < 0.5
    slot_buf[...] = jnp.where(right_slot, named, 0.0).T.astype(BF16)
    scaled = jnp.where(right_slot, scaled, 0.0)
    high = scaled.astype(BF16)
    weight_buf[0] = high
    weight_buf[1] = (scaled - high.astype(F32)).astype(BF16)
    gelu_buf[...] = jax.nn.gelu(gatein[...].astype(F32))

    for d in FAR_FIRST:
        got = carry1.at[(pi + PLANE - d) % PLANE]
        remote(got, got, carry_sem, (0, d), sp, tp).wait_recv()
    one = jnp.ones((4, 128), F32)
    nought = jnp.zeros((4, 128), F32)
    all_p, all_s, in_p, in_s = one, nought, one, nought
    for j in range(PLANE):
        p_j, s_j = carry1[j, 0], carry1[j, 1]
        all_p, all_s = all_p * p_j, p_j * all_s + s_j
        in_p = jnp.where(j < pi, in_p * p_j, in_p)
        in_s = jnp.where(j < pi, p_j * in_s + s_j, in_s)
    mine2 = carry2.at[zi]
    mine2[0] = all_p
    mine2[1] = all_s
    for d in FAR_FIRST:
        send(mine2, mine2, carry_sem, (1, d), z_peer(d), tp)
    for d in FAR_FIRST:
        got = carry2.at[(zi + PLANES - d) % PLANES]
        remote(got, got, carry_sem, (1, d), sp, tp).wait_recv()
    planes_s = nought
    for k in range(PLANES):
        planes_s = jnp.where(k < zi, carry2[k, 0] * planes_s + carry2[k, 1], planes_s)
    carry_in = in_p * planes_s + in_s
    carry_row = jnp.concatenate([carry_in[b : b + 1] for b in range(4)], axis=1)
    carry_tail = head_s + head_p * carry_row
    states = cum_s[:HEAD_ROWS] + cum_p[:HEAD_ROWS] * carry_row
    branch[:HEAD_ROWS, :] = (gelu_buf[:HEAD_ROWS] * states).astype(BF16)
    states = cum_s[HEAD_ROWS:] + cum_p[HEAD_ROWS:] * carry_tail
    branch[HEAD_ROWS:, :] = (gelu_buf[HEAD_ROWS:] * states).astype(BF16)

    loads[10].wait()
    for c in range(4):
        cols = slice(512 * c, 512 * c + 512)
        value = dot(branch[...], wout[:, cols]).astype(BF16)
        part[:, :, cols] = value.reshape(TPS, 32, 512)
        for d in (2, 1, 3):
            to = (tp + d) % TPS
            send(part.at[to, :, cols], mixed_buf.at[tp, :, cols], mix_sem, (c, d), sp, to)
    for k in (8, 9):
        loads[k].wait()
    weights_out(up_w, tp, left, 2)
    weights_out(up_w, tp, right, 3)
    weights_in(gate_w, right, 0)
    weights_in(gate_w, left, 1)
    weights_out(gate_w, right, left, 4)
    for k in (13, 14, 15):
        loads[k].wait()
    for c in range(4):
        cols = slice(512 * c, 512 * c + 512)
        for d in (2, 1, 3):
            came = (tp + TPS - d) % TPS
            got = mixed_buf.at[came, :, cols]
            remote(got, got, mix_sem, (c, d), sp, tp).wait_recv()
    mixed = part[tp].astype(F32)
    for d in (1, 2, 3):
        mixed = mixed + mixed_buf[(tp + d) % TPS].astype(F32)
    normed[...] = layer_norm(
        RESIDUAL_SCALE * stream[...].astype(F32) + mixed, gain1[...], bias1[...]
    ).astype(BF16)

    width = 2048 // CHUNKS

    def exchange(src, dst, sem, hop, c, me, peer):
        cols = slice(width * c, width * c + width)
        size = src.shape[0]
        for d in FAR_FIRST:
            to = (me + d) % size
            send(src.at[to, :, cols], dst.at[me, :, cols], sem, (hop, c, d), peer(d), tp)
        dst[me, :, cols] = src[me, :, cols]

    def arrived(dst, sem, hop, c, me):
        cols = slice(width * c, width * c + width)
        size = dst.shape[0]
        for d in FAR_FIRST:
            got = dst.at[(me + size - d) % size, :, cols]
            remote(got, got, sem, (hop, c, d), sp, tp).wait_recv()

    def swapped(src, c):
        cols = slice(width * c, width * c + width)
        to_row = lax.broadcasted_iota(jnp.int32, (128, 128), 0)
        from_row = lax.broadcasted_iota(jnp.int32, (128, 128), 1)
        outer, inner, pair = to_row // 16, (to_row // 2) % 8, to_row % 2
        pick = (from_row == inner * 16 + outer * 2 + pair).astype(BF16)
        rows = src[:, :, cols].reshape(128, width)
        return dot(pick, rows).astype(BF16).reshape(8, 16, width)

    for c in range(CHUNKS):
        cols = slice(width * c, width * c + width)
        value = dot(slot_buf[...], normed[:, cols]).astype(BF16)
        disp[:, :, cols] = value.reshape(8, 16, width)
        exchange(disp, arr1, disp_sem, 0, c, zi, z_peer)
    weights_out(down_w, tp, left, 6)
    weights_in(up_w, left, 3)
    weights_out(up_w, left, right, 5)
    weights_out(down_w, tp, right, 7)

    for k in (16, 17, 18, 19, 20):
        loads[k].wait()
    rows = normed[...]
    hidden = jax.nn.silu(dot(rows, shared_gate[...])) * dot(rows, shared_up[...])
    acc[...] = RESIDUAL_SCALE * rows.astype(F32) + dot(hidden.astype(BF16), shared_down[...])

    for c in range(CHUNKS):
        cols = slice(width * c, width * c + width)
        arrived(arr1, disp_sem, 0, c, zi)
        disp2[:, :, cols] = swapped(arr1, c)
        exchange(disp2, arr2, disp_sem, 1, c, pi, plane_peer)

    for c in range(CHUNKS):
        arrived(arr2, disp_sem, 1, c, pi)
    weights_in(up_w, right, 2)
    picked = arr2[...].reshape(128, 2048)
    weights_in(gate_w, opposite, 4)
    gated = [dot(picked, gate_w[k]) for k in range(TPS)]
    weights_in(up_w, opposite, 5)
    lifted = [dot(picked, up_w[k]) for k in range(TPS)]
    hidden = jnp.concatenate(
        [(jax.nn.silu(g) * u).astype(BF16) for g, u in zip(gated, lifted)], axis=1
    )
    half = 64
    weights_in(down_w, right, 6)
    right_half = down_w.at[right, :half]
    send(right_half, right_half, weight_sem, (8,), sp, left)
    weights_in(down_w, left, 7)
    left_half = down_w.at[left, half:]
    send(left_half, left_half, weight_sem, (9,), sp, right)
    low, high = down_w.at[opposite, :half], down_w.at[opposite, half:]
    remote(low, low, weight_sem, (8,), sp, left).wait_recv()
    remote(high, high, weight_sem, (9,), sp, left).wait_recv()
    for c in range(CHUNKS):
        cols = slice(width * c, width * c + width)
        value = dot(hidden, down_w[:, :, cols].reshape(512, width)).astype(BF16)
        moe_out[:, :, cols] = value.reshape(8, 16, width)
        exchange(moe_out, ret1, ret_sem, 0, c, pi, plane_peer)

    for c in range(CHUNKS):
        cols = slice(width * c, width * c + width)
        arrived(ret1, ret_sem, 0, c, pi)
        ret1p[:, :, cols] = swapped(ret1, c)
        exchange(ret1p, ret2, ret_sem, 1, c, zi, z_peer)
    for c in range(CHUNKS):
        cols = slice(width * c, width * c + width)
        arrived(ret2, ret_sem, 1, c, zi)
        back = ret2[:, :, cols].reshape(128, width)
        acc[:, cols] = acc[:, cols] + dot(weight_buf[0], back) + dot(weight_buf[1], back)
    out_ref[...] = layer_norm(acc[...], gain2[...], bias2[...]).astype(BF16)
    for copy in sends:
        copy.wait_send()


def shards(
    stream, recurrence_input, output_gate_input, convolution_taps, first_group_gates,
    second_group_gates, channel_decay, position_log_extra, recurrence_output_weight,
    first_norm_gain, first_norm_bias, routed_expert_index, routed_expert_weight,
    routed_gate_weight, routed_up_weight, routed_down_weight, shared_gate_weight,
    shared_up_weight, shared_down_weight, second_norm_gain, second_norm_bias,
):
    operands = (
        stream,
        recurrence_input.reshape(128, 512),
        output_gate_input.reshape(128, 512),
        convolution_taps.reshape(4, 512),
        first_group_gates,
        second_group_gates,
        channel_decay.reshape(1, 512),
        position_log_extra.reshape(128, 512),
        recurrence_output_weight.reshape(512, 2048),
        first_norm_gain.reshape(1, 2048),
        first_norm_bias.reshape(1, 2048),
        routed_expert_index,
        routed_expert_weight,
        routed_gate_weight.reshape(2048, 128),
        routed_up_weight.reshape(2048, 128),
        routed_down_weight.reshape(128, 2048),
        shared_gate_weight,
        shared_up_weight,
        shared_down_weight,
        second_norm_gain.reshape(1, 2048),
        second_norm_bias.reshape(1, 2048),
    )
    gathered = {13: (4, 2048, 128), 14: (4, 2048, 128), 15: (4, 128, 2048)}
    held = [
        pltpu.VMEM(gathered.get(k, operand.shape), operand.dtype)
        for k, operand in enumerate(operands)
    ]
    wide = pltpu.VMEM((8, 16, 2048), BF16)
    return pl.pallas_call(
        mega,
        out_shape=jax.ShapeDtypeStruct((32, 2048), BF16),
        in_specs=[pl.BlockSpec(memory_space=pl.ANY)] * len(operands),
        out_specs=pl.BlockSpec(memory_space=pltpu.VMEM),
        scratch_shapes=[
            *held,
            pltpu.VMEM((128 + HEAD_ROWS, 512), F32),
            pltpu.VMEM((HEAD_ROWS, 512), BF16),
            pltpu.VMEM((128, 512), F32),
            pltpu.VMEM((128, 512), F32),
            pltpu.VMEM((PLANE, 2, 4, 128), F32),
            pltpu.VMEM((PLANES, 2, 4, 128), F32),
            pltpu.VMEM((128, 512), F32),
            pltpu.VMEM((128, 512), BF16),
            pltpu.VMEM((TPS, 32, 2048), BF16),
            pltpu.VMEM((TPS, 32, 2048), BF16),
            pltpu.VMEM((32, 2048), BF16),
            pltpu.VMEM((128, 32), BF16),
            pltpu.VMEM((2, 32, 128), BF16),
            wide, wide, wide, wide, wide, wide, wide, wide,
            pltpu.VMEM((32, 2048), F32),
            pltpu.SemaphoreType.DMA((len(operands),)),
            pltpu.SemaphoreType.DMA((2,)),
            pltpu.SemaphoreType.DMA((2,)),
            pltpu.SemaphoreType.DMA((2, 10)),
            pltpu.SemaphoreType.DMA((2, 2, 8)),
            pltpu.SemaphoreType.DMA((2, 4, 4)),
            pltpu.SemaphoreType.DMA((2, 2, CHUNKS, 8)),
            pltpu.SemaphoreType.DMA((2, 2, CHUNKS, 8)),
        ],
        compiler_params=pltpu.CompilerParams(
            collective_id=0, has_side_effects=True, vmem_limit_bytes=56 * 2**20
        ),
        name="mega",
    )(*operands)


def solution(mesh):
    in_specs = (
        P(("sp", "tp"), None),
        P("sp", None, "tp"),
        P("sp", None, "tp"),
        P(None, None, "tp"),
        P(None, "tp", None, None),
        P(None, "tp", None, None),
        P(None, "tp"),
        P("sp", None, "tp"),
        P(None, "tp", None),
        P(),
        P(),
        P("sp", None),
        P("sp", None),
        P("sp", None, "tp"),
        P("sp", None, "tp"),
        P("sp", "tp", None),
        P(),
        P(),
        P(),
        P(),
        P(),
    )
    out_specs = P(("sp", "tp"), None)
    return jax.shard_map(shards, mesh=mesh, in_specs=in_specs, out_specs=out_specs, check_vma=False)
```

time: 207 us -> 104 us (0.50)
  Pallas kernels: 0 us -> 92.2 us
  waiting for transfers between devices: 58.8 us -> 0 us
  blocking collectives: 52.1 us -> 0 us
  starting transfers between devices: 32 us -> 0 us
  matrix products: 15.4 us -> 0 us
  between operations: 14.3 us -> 0.01 us
  other arithmetic: 13.3 us -> 0 us
  local copies, waits for them, and re-layouts: 19.8 us -> 11.7 us
    pallas_call x0 -> x1, Pallas kernels: none -> 92.2 us  [shards(): pl.pallas_call(mega, out_shape=jax.ShapeDtypeStruct((32, 2048), BF16), in...]
    all_to_all x2 -> x0, blocking collectives: 52.1 us -> none  [the longest x1 28.9 us: summed_on_arrival(): lax.all_to_all(cut_along(shard, dim, count), axis, 0, 0, tiled=True)]
    all_to_all x3 -> x0, waiting for transfers between devices: 31 us -> none  [the longest x1 14.8 us: shards(): lax.all_to_all(leaving, 'sp', split_axis=0, concat_axis=0, tiled=True)]
    all_gather x1 -> x0, waiting for transfers between devices: 27.8 us -> none  [shards(): fanned = lax.all_gather(arrived[None], 'tp', axis=0, tiled=True)]
    all_to_all x3 -> x0, starting transfers between devices: 27.5 us -> none  [the longest x1 11.9 us: shards(): lax.all_to_all(leaving, 'sp', split_axis=0, concat_axis=0, tiled=True)]
    dot_general x7 -> x0, matrix products: 15.4 us -> none  [the longest x1 5.22 us: expert_terms(): jnp.einsum(down_form, hidden, down_w, preferred_element_type=jnp.float32)]
    unnamed x46 -> x8, local copies, waits for them, and re-layouts: 2.03 us -> 11.7 us
    ppermute x1 -> x0, starting transfers between devices: 4.5 us -> none  [shifted(): return lax.ppermute(shard, axis, pairs)]
  transfers between devices with their start and end apart: 5 -> 0, of which waited for: 4 -> 0; matrix products, arithmetic and copies ran while one was open for 6% -> 0% of each run, Pallas kernels for 0% -> 0%
where the time goes in v1:
time: 104 us
  Pallas kernels  92.2 us (89%)
  local copies, waits for them, and re-layouts  11.7 us (11%)
    pallas_call x1, Pallas kernels, shards(): pl.pallas_call(mega, out_shape=jax.ShapeDtypeStruct((32, 2048), BF16), in...  92.2 us
    unnamed x8, local copies, waits for them, and re-layouts  11.7 us

profile of v1, /device:TPU:1, one launch (start us, length us, event | category | flops | bytes accessed | tf_op | source)
XLA Modules:
  0.0 104.0 jit_solution(6484363155263953012)
XLA Ops:
  0.0 1.3 %copy.27 = f32[1,1,2,256]{3,1,2,0:T(1,128)} copy(f32[1,1,2,256]{3,2,1,0:T(2,128)} %bitcast.36) | data formatting | bytes 4096
  1.3 1.3 %copy.26 = bf16[1,4,2,256]{3,1,2,0:T(4,128)(2,1)} copy(bf16[1,4,2,256]{3,2,1,0:T(2,128)(2,1)} %bitcast.35) | data formatting | bytes 8192
  2.5 1.4 %copy.22.index_h = s32[128,4]{1,0:T(8,128)} copy(s32[128,4]{0,1:T(4,128)} %param.32) | data formatting | bytes 4096 | tf_op args[11]
  3.9 1.4 %copy.23.weight_h = f32[128,4]{1,0:T(8,128)} copy(f32[128,4]{0,1:T(4,128)} %param.33) | data formatting | bytes 4096 | tf_op args[12]
  5.3 1.6 %copy.24 = bf16[16,8,2,256]{3,1,2,0:T(8,128)(2,1)} copy(bf16[16,8,2,256]{3,2,1,0:T(2,128)(2,1)} %bitcast.27) | data formatting | bytes 262144
  6.9 1.6 %copy.25 = bf16[16,8,2,256]{3,1,2,0:T(8,128)(2,1)} copy(bf16[16,8,2,256]{3,2,1,0:T(2,128)(2,1)} %bitcast.28) | data formatting | bytes 262144
  8.5 1.7 %copy.28 = f32[16,8,2,256]{3,1,2,0:T(8,128)} copy(f32[16,8,2,256]{3,2,1,0:T(2,128)} %bitcast.26) | data formatting | bytes 524288
  10.1 92.2 %mega.1 = bf16[32,2048]{1,0:T(8,128)(2,1)} custom-call(bf16[32,2048]{1,0:T(8,128)(2,1)} %stream_h.1, bf16[128,512]{1,0:T(8,128)(2,1)} %bitcast.21, bf16[128,512]{1,0:T(8,128)(2,1)} %bitcast.22, bf16[4,512]{1,0:T(4,128)(2,1)} %bitcast.29, bf16[2,4,64,64]{3,2,1,0:T(8,128)(2,1)} %small_gates_h.1, bf16[2,2,128,128]{3,2,1,0:T(8,128)(2,1)} %large_gates_h.1, ...), custom_call_target="tpu_custom_call" | custom-call | tf_op jit(solution)/shard_map/mega/pallas_call | solution.py:420
  102.4 1.6 %copy.30 = bf16[32,2048]{1,0:T(8,128)(2,1)} copy(bf16[32,2048]{1,0:T(8,128)(2,1)} %mega.1) | data formatting | bytes 262144

commit v2 on v1

--- a/solution.py
+++ b/solution.py
@@ -17,6 +17,19 @@
 HEAD_ROWS = 16
 CHUNKS = 2
 FAR_FIRST = (4, 3, 5, 2, 6, 1, 7)
+
+
+class Phases:
+    def __init__(self):
+        self.scope = None
+
+    def __call__(self, name=None):
+        if self.scope is not None:
+            self.scope.__exit__(None, None, None)
+        self.scope = None
+        if name is not None:
+            self.scope = jax.named_scope(name)
+            self.scope.__enter__()
 
 
 def layer_norm(values, gain_vec, bias_vec):
@@ -52,10 +65,10 @@
     wout_h, gain1_h, bias1_h, index_h, weight_h, gate_w_h, up_w_h, down_w_h,
     shared_gate_h, shared_up_h, shared_down_h, gain2_h, bias2_h,
     out_ref,
-    stream, rec, gatein, taps, small_gates, large_gates, decay, extra,
+    stream, rec, gatein, taps, small_gates, large_gates, decay, extra_raw,
     wout, gain1, bias1, index, weight, gate_w, up_w, down_w,
     shared_gate, shared_up, shared_down, gain2, bias2,
-    rec_f, border, cum_p, cum_s, carry1, carry2, gelu_buf, branch,
+    extra, turned, rec_f, border, cum_p, cum_s, carry1, carry2, gelu_buf, branch,
     part, mixed_buf, normed, slot_buf, weight_buf,
     disp, arr1, disp2, arr2, moe_out, ret1, ret1p, ret2, acc,
     load_sem, own_sem, border_sem, weight_sem, carry_sem, mix_sem, disp_sem, ret_sem,
@@ -65,6 +78,8 @@
     zi = sp // PLANE
     pi = sp % PLANE
     sends = []
+    phase = Phases()
+    phase("loads")
 
     def load(k, src, dst):
         copy = pltpu.make_async_copy(src, dst, load_sem.at[k])
@@ -95,7 +110,7 @@
 
     names = (
         (rec_h, rec), (small_gates_h, small_gates), (large_gates_h, large_gates), (taps_h, taps),
-        (decay_h, decay), (extra_h, extra), (gatein_h, gatein), (gate_w_h, gate_w.at[tp]),
+        (decay_h, decay), (extra_h, extra_raw), (gatein_h, gatein), (gate_w_h, gate_w.at[tp]),
         (up_w_h, up_w.at[tp]), (down_w_h, down_w.at[tp]), (wout_h, wout), (index_h, index),
         (weight_h, weight), (stream_h, stream), (gain1_h, gain1), (bias1_h, bias1),
         (shared_gate_h, shared_gate), (shared_up_h, shared_up), (shared_down_h, shared_down),
@@ -118,10 +133,14 @@
         greet(sp, (tp + d) % TPS)
     greet((sp + 63) % 64, tp)
 
+    phase("wait_loads")
     for k in range(6):
         loads[k].wait()
     length = rec.shape[0]
-    rec_f[HEAD_ROWS:, :] = rec[...].astype(F32)
+    phase("prepare")
+    for g in range(2):
+        rec_f[HEAD_ROWS:, 256 * g : 256 * g + 256] = rec[:, g, :].astype(F32)
+        extra[:, 256 * g : 256 * g + 256] = extra_raw[:, g, :]
     row_i = lax.broadcasted_iota(jnp.int32, (64, 128), 0)
     col_i = lax.broadcasted_iota(jnp.int32, (64, 128), 1)
     put_low = (row_i == col_i).astype(BF16)
@@ -139,17 +158,20 @@
     rate = -8.0 * softplus_of_minus(decay[...])
     tap_f = taps[...].astype(F32)
 
+    def tap(k, b):
+        return tap_f[k, b // 2 : b // 2 + 1, 128 * (b % 2) : 128 * (b % 2) + 128]
+
     def scanned(first, count):
         for b in range(4):
             lanes = slice(128 * b, 128 * b + 128)
-            conv = tap_f[0:1, lanes] * rec_f[first + HEAD_ROWS - 3 : first + HEAD_ROWS - 3 + count, lanes]
+            conv = tap(0, b) * rec_f[first + HEAD_ROWS - 3 : first + HEAD_ROWS - 3 + count, lanes]
             for k in range(1, 4):
                 at = first + HEAD_ROWS - 3 + k
-                conv = conv + tap_f[k : k + 1, lanes] * rec_f[at : at + count, lanes]
+                conv = conv + tap(k, b) * rec_f[at : at + count, lanes]
             conv = conv.astype(BF16)
             recur_gate = jax.nn.sigmoid(dot(conv, blocks[0][b]))
             input_gate = jax.nn.sigmoid(dot(conv, blocks[1][b]))
-            log_decay = recur_gate * rate[:, lanes] + extra[first : first + count, lanes]
+            log_decay = recur_gate * rate[b // 2 : b // 2 + 1, 128 * (b % 2) : 128 * (b % 2) + 128] + extra[first : first + count, lanes]
             p = jnp.exp(log_decay)
             s = jnp.sqrt(minus_expm1(2.0 * log_decay)) * input_gate * conv.astype(F32)
             p = p.reshape(count // 8, 8, 128)
@@ -170,7 +192,9 @@
                 s_in = s_t[7:8]
                 p_in = p_t[7:8]
 
+    phase("scan_tail")
     scanned(HEAD_ROWS, length - HEAD_ROWS)
+    phase("barrier")
 
     pl.semaphore_wait(barrier, 7 + 7 + 3 + 1)
     send(rec.at[length - HEAD_ROWS :], border, border_sem, (), (sp + 1) % 64, tp)
@@ -185,13 +209,19 @@
         remote(buf.at[slot], buf.at[slot], weight_sem, (k,), sp, left).wait_recv()
 
     opposite = (tp + 2) % TPS
+    phase("send_gate")
     loads[7].wait()
     weights_out(gate_w, tp, left, 0)
     weights_out(gate_w, tp, right, 1)
 
+    phase("border")
     remote(rec.at[length - HEAD_ROWS :], border, border_sem, (), sp, tp).wait_recv()
-    border_f = border[...].astype(F32)
-    rec_f[0:HEAD_ROWS, :] = jnp.where(sp > 0, border_f, jnp.zeros_like(border_f))
+    phase("scan_head")
+    for g in range(2):
+        border_f = border[:, g, :].astype(F32)
+        rec_f[0:HEAD_ROWS, 256 * g : 256 * g + 256] = jnp.where(
+            sp > 0, border_f, jnp.zeros_like(border_f)
+        )
     scanned(0, HEAD_ROWS)
 
     head_p = cum_p[HEAD_ROWS - 1 : HEAD_ROWS, :]
@@ -207,11 +237,15 @@
     for d in FAR_FIRST:
         send(mine1, mine1, carry_sem, (0, d), plane_peer(d), tp)
 
+    phase("slots")
     for k in (6, 11, 12):
         loads[k].wait()
     own_rows = pl.ds(pl.multiple_of(tp * 32, 32), 32)
-    ids = index[own_rows, :]
-    factors = weight[own_rows, :]
+    unused = jnp.zeros((4, 128), F32)
+    turned[0] = jnp.concatenate([index[...].astype(F32), unused], axis=0).T
+    turned[1] = jnp.concatenate([weight[...], unused], axis=0).T
+    ids = turned[0, own_rows, :].astype(jnp.int32)
+    factors = turned[1, own_rows, :]
     slot = lax.broadcasted_iota(jnp.int32, (32, 128), 1)
     named = jnp.zeros((32, 128), F32)
     scaled = jnp.zeros((32, 128), F32)
@@ -229,7 +263,9 @@
     high = scaled.astype(BF16)
     weight_buf[0] = high
     weight_buf[1] = (scaled - high.astype(F32)).astype(BF16)
-    gelu_buf[...] = jax.nn.gelu(gatein[...].astype(F32))
+    for g in range(2):
+        gelu_buf[:, 256 * g : 256 * g + 256] = jax.nn.gelu(gatein[:, g, :].astype(F32))
+    phase("carry1")
 
     for d in FAR_FIRST:
         got = carry1.at[(pi + PLANE - d) % PLANE]
@@ -247,9 +283,11 @@
     mine2[1] = all_s
     for d in FAR_FIRST:
         send(mine2, mine2, carry_sem, (1, d), z_peer(d), tp)
+    phase("carry2")
     for d in FAR_FIRST:
         got = carry2.at[(zi + PLANES - d) % PLANES]
         remote(got, got, carry_sem, (1, d), sp, tp).wait_recv()
+    phase("fixup")
     planes_s = nought
     for k in range(PLANES):
         planes_s = jnp.where(k < zi, carry2[k, 0] * planes_s + carry2[k, 1], planes_s)
@@ -261,6 +299,7 @@
     states = cum_s[HEAD_ROWS:] + cum_p[HEAD_ROWS:] * carry_tail
     branch[HEAD_ROWS:, :] = (gelu_buf[HEAD_ROWS:] * states).astype(BF16)
 
+    phase("out_proj")
     loads[10].wait()
     for c in range(4):
         cols = slice(512 * c, 512 * c + 512)
@@ -269,6 +308,7 @@
         for d in (2, 1, 3):
             to = (tp + d) % TPS
             send(part.at[to, :, cols], mixed_buf.at[tp, :, cols], mix_sem, (c, d), sp, to)
+    phase("gate_arrive")
     for k in (8, 9):
         loads[k].wait()
     weights_out(up_w, tp, left, 2)
@@ -276,6 +316,7 @@
     weights_in(gate_w, right, 0)
     weights_in(gate_w, left, 1)
     weights_out(gate_w, right, left, 4)
+    phase("mix_arrive")
     for k in (13, 14, 15):
         loads[k].wait()
     for c in range(4):
@@ -284,6 +325,7 @@
             came = (tp + TPS - d) % TPS
             got = mixed_buf.at[came, :, cols]
             remote(got, got, mix_sem, (c, d), sp, tp).wait_recv()
+    phase("norm1")
     mixed = part[tp].astype(F32)
     for d in (1, 2, 3):
         mixed = mixed + mixed_buf[(tp + d) % TPS].astype(F32)
@@ -317,16 +359,19 @@
         rows = src[:, :, cols].reshape(128, width)
         return dot(pick, rows).astype(BF16).reshape(8, 16, width)
 
+    phase("dispatch")
     for c in range(CHUNKS):
         cols = slice(width * c, width * c + width)
         value = dot(slot_buf[...], normed[:, cols]).astype(BF16)
         disp[:, :, cols] = value.reshape(8, 16, width)
         exchange(disp, arr1, disp_sem, 0, c, zi, z_peer)
+    phase("up_from_left")
     weights_out(down_w, tp, left, 6)
     weights_in(up_w, left, 3)
     weights_out(up_w, left, right, 5)
     weights_out(down_w, tp, right, 7)
 
+    phase("shared")
     for k in (16, 17, 18, 19, 20):
         loads[k].wait()
     rows = normed[...]
@@ -335,21 +380,29 @@
 
     for c in range(CHUNKS):
         cols = slice(width * c, width * c + width)
+        phase(f"disp_z_{c}")
         arrived(arr1, disp_sem, 0, c, zi)
+        phase(f"disp_swap_{c}")
         disp2[:, :, cols] = swapped(arr1, c)
         exchange(disp2, arr2, disp_sem, 1, c, pi, plane_peer)
 
     for c in range(CHUNKS):
+        phase(f"disp_p_{c}")
         arrived(arr2, disp_sem, 1, c, pi)
+    phase("gate_opposite")
     weights_in(up_w, right, 2)
     picked = arr2[...].reshape(128, 2048)
     weights_in(gate_w, opposite, 4)
+    phase("gated")
     gated = [dot(picked, gate_w[k]) for k in range(TPS)]
+    phase("up_opposite")
     weights_in(up_w, opposite, 5)
+    phase("lifted")
     lifted = [dot(picked, up_w[k]) for k in range(TPS)]
     hidden = jnp.concatenate(
         [(jax.nn.silu(g) * u).astype(BF16) for g, u in zip(gated, lifted)], axis=1
     )
+    phase("down_arrive")
     half = 64
     weights_in(down_w, right, 6)
     right_half = down_w.at[right, :half]
@@ -357,28 +410,37 @@
     weights_in(down_w, left, 7)
     left_half = down_w.at[left, half:]
     send(left_half, left_half, weight_sem, (9,), sp, right)
+    phase("down_opposite")
     low, high = down_w.at[opposite, :half], down_w.at[opposite, half:]
     remote(low, low, weight_sem, (8,), sp, left).wait_recv()
     remote(high, high, weight_sem, (9,), sp, left).wait_recv()
     for c in range(CHUNKS):
         cols = slice(width * c, width * c + width)
+        phase(f"down_{c}")
         value = dot(hidden, down_w[:, :, cols].reshape(512, width)).astype(BF16)
         moe_out[:, :, cols] = value.reshape(8, 16, width)
         exchange(moe_out, ret1, ret_sem, 0, c, pi, plane_peer)
 
     for c in range(CHUNKS):
         cols = slice(width * c, width * c + width)
+        phase(f"ret_p_{c}")
         arrived(ret1, ret_sem, 0, c, pi)
+        phase(f"ret_swap_{c}")
         ret1p[:, :, cols] = swapped(ret1, c)
         exchange(ret1p, ret2, ret_sem, 1, c, zi, z_peer)
     for c in range(CHUNKS):
         cols = slice(width * c, width * c + width)
+        phase(f"ret_z_{c}")
         arrived(ret2, ret_sem, 1, c, zi)
+        phase(f"combine_{c}")
         back = ret2[:, :, cols].reshape(128, width)
         acc[:, cols] = acc[:, cols] + dot(weight_buf[0], back) + dot(weight_buf[1], back)
+    phase("norm2")
     out_ref[...] = layer_norm(acc[...], gain2[...], bias2[...]).astype(BF16)
+    phase("drain")
     for copy in sends:
         copy.wait_send()
+    phase()
 
 
 def shards(
@@ -390,18 +452,18 @@
 ):
     operands = (
         stream,
-        recurrence_input.reshape(128, 512),
-        output_gate_input.reshape(128, 512),
-        convolution_taps.reshape(4, 512),
+        recurrence_input,
+        output_gate_input,
+        convolution_taps,
         first_group_gates,
         second_group_gates,
-        channel_decay.reshape(1, 512),
-        position_log_extra.reshape(128, 512),
+        channel_decay,
+        position_log_extra,
         recurrence_output_weight.reshape(512, 2048),
         first_norm_gain.reshape(1, 2048),
         first_norm_bias.reshape(1, 2048),
-        routed_expert_index,
-        routed_expert_weight,
+        routed_expert_index.T,
+        routed_expert_weight.T,
         routed_gate_weight.reshape(2048, 128),
         routed_up_weight.reshape(2048, 128),
         routed_down_weight.reshape(128, 2048),
@@ -424,8 +486,10 @@
         out_specs=pl.BlockSpec(memory_space=pltpu.VMEM),
         scratch_shapes=[
             *held,
+            pltpu.VMEM((128, 512), F32),
+            pltpu.VMEM((2, 128, 8), F32),
             pltpu.VMEM((128 + HEAD_ROWS, 512), F32),
-            pltpu.VMEM((HEAD_ROWS, 512), BF16),
+            pltpu.VMEM((HEAD_ROWS, 2, 256), BF16),
             pltpu.VMEM((128, 512), F32),
             pltpu.VMEM((128, 512), F32),
             pltpu.VMEM((PLANE, 2, 4, 128), F32),

time: 104 us -> 93.8 us (0.902)
  local copies, waits for them, and re-layouts: 11.7 us -> 1.57 us
    unnamed x8 -> x1, local copies, waits for them, and re-layouts: 11.7 us -> 1.57 us
where the time goes in v2:
time: 93.8 us; the launch traced here: 93.7 us
  Pallas kernels  92.1 us (98%)
  local copies, waits for them, and re-layouts  1.57 us (2%)
    pallas_call x1, Pallas kernels, shards(): pl.pallas_call(mega, out_shape=jax.ShapeDtypeStruct((32, 2048), BF16), in...  92.1 us

profile of v2, /device:TPU:1, one launch (start us, length us, event | category | flops | bytes accessed | tf_op | source)
XLA Modules:
  0.0 93.7 jit_solution(4581708824582363053)
XLA Ops:
  0.0 92.1 %mega.1 = bf16[32,2048]{1,0:T(8,128)(2,1)} custom-call(bf16[32,2048]{1,0:T(8,128)(2,1)} %stream_h.1, bf16[128,2,256]{2,1,0:T(2,128)(2,1)} %rec_h.1, bf16[128,2,256]{2,1,0:T(2,128)(2,1)} %gatein_h.1, bf16[4,2,256]{2,1,0:T(2,128)(2,1)} %taps_h.1, bf16[2,4,64,64]{3,2,1,0:T(8,128)(2,1)} %small_gates_h.1, bf16[2,2,128,128]{3,2,1,0:T(8,128)(2,1)} %large_gates_h.1, ...), custom_call_target="tpu_custom_call" | custom-call | tf_op jit(solution)/shard_map/mega/pallas_call | solution.py:482
  92.1 1.6 %copy.23 = bf16[32,2048]{1,0:T(8,128)(2,1)} copy(bf16[32,2048]{1,0:T(8,128)(2,1)} %mega.1) | data formatting | bytes 262144

commit v3 on v2

--- a/solution.py
+++ b/solution.py
@@ -71,12 +71,21 @@
     extra, turned, rec_f, border, cum_p, cum_s, carry1, carry2, gelu_buf, branch,
     part, mixed_buf, normed, slot_buf, weight_buf,
     disp, arr1, disp2, arr2, moe_out, ret1, ret1p, ret2, acc,
-    load_sem, own_sem, border_sem, weight_sem, carry_sem, mix_sem, disp_sem, ret_sem,
+    own_gate, own_up, own_down,
+    load_sem, slot_sem, border_sem, weight_sem, carry_sem, mix_sem, disp_sem, ret_sem,
 ):
     sp = lax.axis_index("sp")
     tp = lax.axis_index("tp")
     zi = sp // PLANE
     pi = sp % PLANE
+    xi = pi // 2
+    core = sp % 2
+    hosted = tp // 2
+    mirror = 3 - tp
+    mate = tp + 1 - 2 * (tp % 2)
+    sibling = sp + 1 - 2 * core
+    owner = core == hosted
+    guest = core != hosted
     sends = []
     phase = Phases()
     phase("loads")
@@ -86,21 +95,24 @@
         copy.start()
         return copy
 
-    def remote(src, dst, sem, where, sp_to, tp_to):
+    def remote(src, dst, sem, where, sp_to, tp_to, lands=None):
         copy = pltpu.make_async_remote_copy(
             src_ref=src,
             dst_ref=dst,
             send_sem=sem.at[(0, *where)],
-            recv_sem=sem.at[(1, *where)],
+            recv_sem=sem.at[(1, *(lands or where))],
             device_id={"sp": sp_to, "tp": tp_to},
             device_id_type=MESH,
         )
         return copy
 
-    def send(*args):
-        copy = remote(*args)
-        copy.start()
-        sends.append(copy)
+    def send(*args, lands=None, when=None):
+        copy = remote(*args, lands=lands)
+        if when is None:
+            copy.start()
+        else:
+            pl.when(when)(copy.start)
+        sends.append((copy, when))
 
     def plane_peer(d):
         return zi * PLANE + (pi + d) % PLANE
@@ -110,13 +122,24 @@
 
     names = (
         (rec_h, rec), (small_gates_h, small_gates), (large_gates_h, large_gates), (taps_h, taps),
-        (decay_h, decay), (extra_h, extra_raw), (gatein_h, gatein), (gate_w_h, gate_w.at[tp]),
-        (up_w_h, up_w.at[tp]), (down_w_h, down_w.at[tp]), (wout_h, wout), (index_h, index),
+        (decay_h, decay), (extra_h, extra_raw), (gatein_h, gatein), (gate_w_h, own_gate),
+        (up_w_h, own_up), (down_w_h, own_down), (wout_h, wout), (index_h, index),
         (weight_h, weight), (stream_h, stream), (gain1_h, gain1), (bias1_h, bias1),
         (shared_gate_h, shared_gate), (shared_up_h, shared_up), (shared_down_h, shared_down),
         (gain2_h, gain2), (bias2_h, bias2),
     )
     loads = [load(k, src, dst) for k, (src, dst) in enumerate(names)]
+    owns = (own_gate, own_up, own_down)
+    wholes = (gate_w, up_w, down_w)
+    slot_loads = [
+        pltpu.make_async_copy(src, dst.at[tp], slot_sem.at[m])
+        for m, (src, dst) in enumerate(zip((gate_w_h, up_w_h, down_w_h), wholes))
+    ]
+
+    @pl.when(owner)
+    def _():
+        for copy in slot_loads:
+            copy.start()
 
     barrier = pltpu.get_barrier_semaphore()
 
@@ -132,6 +155,8 @@
     for d in range(1, TPS):
         greet(sp, (tp + d) % TPS)
     greet((sp + 63) % 64, tp)
+    for j in range(PLANE):
+        greet(zi * PLANE + j, mirror)
 
     phase("wait_loads")
     for k in range(6):
@@ -196,23 +221,35 @@
     scanned(HEAD_ROWS, length - HEAD_ROWS)
     phase("barrier")
 
-    pl.semaphore_wait(barrier, 7 + 7 + 3 + 1)
+    pl.semaphore_wait(barrier, 7 + 7 + 3 + 1 + 8)
     send(rec.at[length - HEAD_ROWS :], border, border_sem, (), (sp + 1) % 64, tp)
 
-    left = (tp + 3) % TPS
-    right = (tp + 1) % TPS
-
-    def weights_out(buf, slot, to, k):
-        send(buf.at[slot], buf.at[slot], weight_sem, (k,), sp, to)
-
-    def weights_in(buf, slot, k):
-        remote(buf.at[slot], buf.at[slot], weight_sem, (k,), sp, left).wait_recv()
-
-    opposite = (tp + 2) % TPS
+    far = 3 - mate
+    FROM_MATE, FROM_MIRROR, FROM_FAR, OWN, MATE, MIRROR, FAR = range(7)
+    slots = {
+        FROM_MATE: mate, FROM_MIRROR: mirror, FROM_FAR: far,
+        OWN: tp, MATE: mate, MIRROR: mirror, FAR: far,
+    }
+
+    def part_out(src, m, at, kind, sp_to, tp_to, when):
+        send(src, wholes[m].at[at], weight_sem, (kind, m), sp_to, tp_to, when=when)
+
+    def part_in(m, kind):
+        got = wholes[m].at[slots[kind]]
+        remote(got, got, weight_sem, (kind, m), sp, tp).wait_recv()
+
+    def pass_on(m, kind, to_sibling):
+        got = wholes[m].at[slots[kind]]
+        part_out(got, m, slots[kind], to_sibling, sibling, tp, owner)
+
     phase("send_gate")
-    loads[7].wait()
-    weights_out(gate_w, tp, left, 0)
-    weights_out(gate_w, tp, right, 1)
+    for k in (7, 8, 9):
+        loads[k].wait()
+    for m in (0, 1):
+        part_out(owns[m], m, tp, FROM_MATE, sp, mate, owner)
+        part_out(owns[m], m, tp, FROM_MIRROR, sp, mirror, guest)
+    for m in (0, 1, 2):
+        part_out(owns[m], m, tp, OWN, sibling, tp, owner)
 
     phase("border")
     remote(rec.at[length - HEAD_ROWS :], border, border_sem, (), sp, tp).wait_recv()
@@ -309,13 +346,24 @@
             to = (tp + d) % TPS
             send(part.at[to, :, cols], mixed_buf.at[tp, :, cols], mix_sem, (c, d), sp, to)
     phase("gate_arrive")
-    for k in (8, 9):
-        loads[k].wait()
-    weights_out(up_w, tp, left, 2)
-    weights_out(up_w, tp, right, 3)
-    weights_in(gate_w, right, 0)
-    weights_in(gate_w, left, 1)
-    weights_out(gate_w, right, left, 4)
+    for m in (0, 1):
+
+        @pl.when(owner)
+        def _():
+            part_in(m, FROM_MIRROR)
+
+        mirrored = wholes[m].at[mirror]
+        part_out(mirrored, m, mirror, FROM_FAR, sp, mate, owner)
+        pass_on(m, FROM_MIRROR, MIRROR)
+    part_out(own_down, 2, tp, FROM_MATE, sp, mate, owner)
+    part_out(own_down, 2, tp, FROM_MIRROR, sp, mirror, guest)
+    for m in (0, 1):
+
+        @pl.when(owner)
+        def _():
+            part_in(m, FROM_MATE)
+
+        pass_on(m, FROM_MATE, MATE)
     phase("mix_arrive")
     for k in (13, 14, 15):
         loads[k].wait()
@@ -365,12 +413,6 @@
         value = dot(slot_buf[...], normed[:, cols]).astype(BF16)
         disp[:, :, cols] = value.reshape(8, 16, width)
         exchange(disp, arr1, disp_sem, 0, c, zi, z_peer)
-    phase("up_from_left")
-    weights_out(down_w, tp, left, 6)
-    weights_in(up_w, left, 3)
-    weights_out(up_w, left, right, 5)
-    weights_out(down_w, tp, right, 7)
-
     phase("shared")
     for k in (16, 17, 18, 19, 20):
         loads[k].wait()
@@ -378,53 +420,138 @@
     hidden = jax.nn.silu(dot(rows, shared_gate[...])) * dot(rows, shared_up[...])
     acc[...] = RESIDUAL_SCALE * rows.astype(F32) + dot(hidden.astype(BF16), shared_down[...])
 
+    phase("down_from_mirror")
+
+    @pl.when(owner)
+    def _():
+        part_in(2, FROM_MIRROR)
+
+    part_out(down_w.at[mirror], 2, mirror, FROM_FAR, sp, mate, owner)
+    pass_on(2, FROM_MIRROR, MIRROR)
+
     for c in range(CHUNKS):
         cols = slice(width * c, width * c + width)
         phase(f"disp_z_{c}")
         arrived(arr1, disp_sem, 0, c, zi)
         phase(f"disp_swap_{c}")
         disp2[:, :, cols] = swapped(arr1, c)
-        exchange(disp2, arr2, disp_sem, 1, c, pi, plane_peer)
-
+        for dx in (2, 1, 3, 0):
+            x_to = (xi + dx) % 4
+            for other in (1, 0):
+                expert = hosted + other * (1 - 2 * hosted)
+                send(
+                    disp2.at[x_to * 2 + expert, :, cols],
+                    arr2.at[pi, :, cols],
+                    disp_sem,
+                    (1, c, dx * 2 + other),
+                    zi * PLANE + x_to * 2 + hosted,
+                    mirror if other else tp,
+                    lands=(1, c, dx * 2 + core),
+                    when=guest if dx == 0 and other == 0 else None,
+                )
+
+        @pl.when(owner)
+        def _():
+            arr2[pi, :, cols] = disp2[pi, :, cols]
+
+    phase("far_gate_up")
+    for m in (0, 1):
+
+        @pl.when(owner)
+        def _():
+            part_in(m, FROM_FAR)
+
+        pass_on(m, FROM_FAR, FAR)
     for c in range(CHUNKS):
+        cols = slice(width * c, width * c + width)
         phase(f"disp_p_{c}")
-        arrived(arr2, disp_sem, 1, c, pi)
-    phase("gate_opposite")
-    weights_in(up_w, right, 2)
+        for dx in (2, 1, 3, 0):
+            for source_core in (0, 1):
+                got = arr2.at[((xi + 4 - dx) % 4) * 2 + source_core, :, cols]
+                copy = remote(got, got, disp_sem, (1, c, dx * 2 + source_core), sp, tp)
+                if dx == 0:
+                    pl.when(jnp.logical_or(guest, core != source_core))(copy.wait_recv)
+                else:
+                    copy.wait_recv()
     picked = arr2[...].reshape(128, 2048)
-    weights_in(gate_w, opposite, 4)
+    phase("down_from_mate")
+
+    @pl.when(owner)
+    def _():
+        part_in(2, FROM_MATE)
+
+    pass_on(2, FROM_MATE, MATE)
+    phase("gate_up_guest")
+
+    @pl.when(owner)
+    def _():
+        for copy in slot_loads:
+            copy.wait()
+
+    @pl.when(guest)
+    def _():
+        for m in (0, 1):
+            for kind in (OWN, MATE, MIRROR, FAR):
+                part_in(m, kind)
+
     phase("gated")
     gated = [dot(picked, gate_w[k]) for k in range(TPS)]
-    phase("up_opposite")
-    weights_in(up_w, opposite, 5)
     phase("lifted")
     lifted = [dot(picked, up_w[k]) for k in range(TPS)]
     hidden = jnp.concatenate(
         [(jax.nn.silu(g) * u).astype(BF16) for g, u in zip(gated, lifted)], axis=1
     )
     phase("down_arrive")
-    half = 64
-    weights_in(down_w, right, 6)
-    right_half = down_w.at[right, :half]
-    send(right_half, right_half, weight_sem, (8,), sp, left)
-    weights_in(down_w, left, 7)
-    left_half = down_w.at[left, half:]
-    send(left_half, left_half, weight_sem, (9,), sp, right)
-    phase("down_opposite")
-    low, high = down_w.at[opposite, :half], down_w.at[opposite, half:]
-    remote(low, low, weight_sem, (8,), sp, left).wait_recv()
-    remote(high, high, weight_sem, (9,), sp, left).wait_recv()
+
+    @pl.when(owner)
+    def _():
+        part_in(2, FROM_FAR)
+
+    pass_on(2, FROM_FAR, FAR)
+    phase("down_guest")
+
+    @pl.when(guest)
+    def _():
+        for kind in (OWN, MATE, MIRROR, FAR):
+            part_in(2, kind)
+
     for c in range(CHUNKS):
         cols = slice(width * c, width * c + width)
         phase(f"down_{c}")
         value = dot(hidden, down_w[:, :, cols].reshape(512, width)).astype(BF16)
         moe_out[:, :, cols] = value.reshape(8, 16, width)
-        exchange(moe_out, ret1, ret_sem, 0, c, pi, plane_peer)
+        home = jnp.where(owner, tp, mirror)
+        foreign = jnp.where(owner, 0, 1)
+        for dx in (2, 1, 3, 0):
+            for target_core in (0, 1):
+                j = ((xi + dx) % 4) * 2 + target_core
+                send(
+                    moe_out.at[j, :, cols],
+                    ret1.at[xi * 2 + hosted, :, cols],
+                    ret_sem,
+                    (0, c, dx * 2 + target_core),
+                    zi * PLANE + j,
+                    home,
+                    lands=(0, c, dx * 2 + foreign),
+                    when=jnp.logical_or(guest, core != target_core) if dx == 0 else None,
+                )
+
+        @pl.when(owner)
+        def _():
+            ret1[pi, :, cols] = moe_out[pi, :, cols]
 
     for c in range(CHUNKS):
         cols = slice(width * c, width * c + width)
         phase(f"ret_p_{c}")
-        arrived(ret1, ret_sem, 0, c, pi)
+        for dx in (2, 1, 3, 0):
+            for other in (1, 0):
+                expert = hosted + other * (1 - 2 * hosted)
+                got = ret1.at[((xi + 4 - dx) % 4) * 2 + expert, :, cols]
+                copy = remote(got, got, ret_sem, (0, c, dx * 2 + other), sp, tp)
+                if dx == 0 and other == 0:
+                    pl.when(guest)(copy.wait_recv)
+                else:
+                    copy.wait_recv()
         phase(f"ret_swap_{c}")
         ret1p[:, :, cols] = swapped(ret1, c)
         exchange(ret1p, ret2, ret_sem, 1, c, zi, z_peer)
@@ -438,8 +565,11 @@
     phase("norm2")
     out_ref[...] = layer_norm(acc[...], gain2[...], bias2[...]).astype(BF16)
     phase("drain")
-    for copy in sends:
-        copy.wait_send()
+    for copy, when in sends:
+        if when is None:
+            copy.wait_send()
+        else:
+            pl.when(when)(copy.wait_send)
     phase()
 
 
@@ -503,10 +633,13 @@
             pltpu.VMEM((2, 32, 128), BF16),
             wide, wide, wide, wide, wide, wide, wide, wide,
             pltpu.VMEM((32, 2048), F32),
+            pltpu.VMEM((2048, 128), BF16),
+            pltpu.VMEM((2048, 128), BF16),
+            pltpu.VMEM((128, 2048), BF16),
             pltpu.SemaphoreType.DMA((len(operands),)),
+            pltpu.SemaphoreType.DMA((3,)),
             pltpu.SemaphoreType.DMA((2,)),
-            pltpu.SemaphoreType.DMA((2,)),
-            pltpu.SemaphoreType.DMA((2, 10)),
+            pltpu.SemaphoreType.DMA((2, 7, 3)),
             pltpu.SemaphoreType.DMA((2, 2, 8)),
             pltpu.SemaphoreType.DMA((2, 4, 4)),
             pltpu.SemaphoreType.DMA((2, 2, CHUNKS, 8)),

time: 93.8 us -> 78.4 us (0.84)
  Pallas kernels: 92.1 us -> 76.7 us
    pallas_call x1, Pallas kernels: 92.1 us -> 76.7 us  [shards(): pl.pallas_call(mega, out_shape=jax.ShapeDtypeStruct((32, 2048), BF16), in...]
where the time goes in v3:
time: 78.4 us; the launch traced here: 78.3 us
  Pallas kernels  76.7 us (98%)
  local copies, waits for them, and re-layouts  1.57 us (2%)
    pallas_call x1, Pallas kernels, shards(): pl.pallas_call(mega, out_shape=jax.ShapeDtypeStruct((32, 2048), BF16), in...  76.7 us
    unnamed x1, local copies, waits for them, and re-layouts  1.57 us

profile of v3, /device:TPU:1, one launch (start us, length us, event | category | flops | bytes accessed | tf_op | source)
XLA Modules:
  0.0 78.3 jit_solution(363049273951665037)
XLA Ops:
  0.0 76.7 %mega.1 = bf16[32,2048]{1,0:T(8,128)(2,1)} custom-call(bf16[32,2048]{1,0:T(8,128)(2,1)} %stream_h.1, bf16[128,2,256]{2,1,0:T(2,128)(2,1)} %rec_h.1, bf16[128,2,256]{2,1,0:T(2,128)(2,1)} %gatein_h.1, bf16[4,2,256]{2,1,0:T(2,128)(2,1)} %taps_h.1, bf16[2,4,64,64]{3,2,1,0:T(8,128)(2,1)} %small_gates_h.1, bf16[2,2,128,128]{3,2,1,0:T(8,128)(2,1)} %large_gates_h.1, ...), custom_call_target="tpu_custom_call" | custom-call | tf_op jit(solution)/shard_map/mega/pallas_call | solution.py:612
  76.7 1.6 %copy.23 = bf16[32,2048]{1,0:T(8,128)(2,1)} copy(bf16[32,2048]{1,0:T(8,128)(2,1)} %mega.1) | data formatting | bytes 262144

commit v4 on v2

--- a/solution.py
+++ b/solution.py
@@ -15,7 +15,7 @@
 PLANES = 8
 TPS = 4
 HEAD_ROWS = 16
-CHUNKS = 2
+CHUNKS = 4
 FAR_FIRST = (4, 3, 5, 2, 6, 1, 7)
 
 
@@ -66,41 +66,53 @@
     shared_gate_h, shared_up_h, shared_down_h, gain2_h, bias2_h,
     out_ref,
     stream, rec, gatein, taps, small_gates, large_gates, decay, extra_raw,
-    wout, gain1, bias1, index, weight, gate_w, up_w, down_w,
+    wout, gain1, bias1, index, weight, own_gate, own_up, own_down,
     shared_gate, shared_up, shared_down, gain2, bias2,
+    gate_up, down_w,
     extra, turned, rec_f, border, cum_p, cum_s, carry1, carry2, gelu_buf, branch,
     part, mixed_buf, normed, slot_buf, weight_buf,
     disp, arr1, disp2, arr2, moe_out, ret1, ret1p, ret2, acc,
-    load_sem, own_sem, border_sem, weight_sem, carry_sem, mix_sem, disp_sem, ret_sem,
+    load_sem, slot_sem, border_sem, part_sem, guest_sem, part_out_sem, carry_sem, mix_sem,
+    z_sem, p_sem, hop_out_sem,
 ):
     sp = lax.axis_index("sp")
     tp = lax.axis_index("tp")
     zi = sp // PLANE
     pi = sp % PLANE
-    sends = []
+    xi = pi // 2
+    core = sp % 2
+    hosted = tp // 2
+    mirror = 3 - tp
+    mate = tp + 1 - 2 * (tp % 2)
+    far = 3 - mate
+    sibling = sp + 1 - 2 * core
+    owner = core == hosted
+    guest = core != hosted
     phase = Phases()
     phase("loads")
 
-    def load(k, src, dst):
-        copy = pltpu.make_async_copy(src, dst, load_sem.at[k])
-        copy.start()
-        return copy
-
-    def remote(src, dst, sem, where, sp_to, tp_to):
-        copy = pltpu.make_async_remote_copy(
+    def remote(src, dst, send_sem, recv_sem, sp_to, tp_to):
+        return pltpu.make_async_remote_copy(
             src_ref=src,
             dst_ref=dst,
-            send_sem=sem.at[(0, *where)],
-            recv_sem=sem.at[(1, *where)],
+            send_sem=send_sem,
+            recv_sem=recv_sem,
             device_id={"sp": sp_to, "tp": tp_to},
             device_id_type=MESH,
         )
-        return copy
-
-    def send(*args):
+
+    def send(*args, when=None):
         copy = remote(*args)
-        copy.start()
-        sends.append(copy)
+        if when is None:
+            copy.start()
+        else:
+            pl.when(when)(copy.start)
+
+    def came(ref, sem):
+        remote(ref, ref, sem, sem, sp, tp).wait_recv()
+
+    def left(ref, sem):
+        remote(ref, ref, sem, sem, sp, tp).wait_send()
 
     def plane_peer(d):
         return zi * PLANE + (pi + d) % PLANE
@@ -108,36 +120,108 @@
     def z_peer(d):
         return ((zi + d) % PLANES) * PLANE + pi
 
+    barrier = pltpu.get_barrier_semaphore()
+
+    def greet(sp_to, tp_to):
+        pl.semaphore_signal(
+            barrier, inc=1, device_id={"sp": sp_to, "tp": tp_to}, device_id_type=MESH
+        )
+
+    for d in FAR_FIRST:
+        greet(z_peer(d), tp)
+    for d in FAR_FIRST:
+        greet(plane_peer(d), tp)
+    for d in range(1, TPS):
+        greet(sp, (tp + d) % TPS)
+    greet((sp + 63) % 64, tp)
+    for j in range(PLANE):
+        greet(zi * PLANE + j, mirror)
+
     names = (
         (rec_h, rec), (small_gates_h, small_gates), (large_gates_h, large_gates), (taps_h, taps),
-        (decay_h, decay), (extra_h, extra_raw), (gatein_h, gatein), (gate_w_h, gate_w.at[tp]),
-        (up_w_h, up_w.at[tp]), (down_w_h, down_w.at[tp]), (wout_h, wout), (index_h, index),
+        (decay_h, decay), (extra_h, extra_raw), (gatein_h, gatein), (gate_w_h, own_gate),
+        (up_w_h, own_up), (down_w_h, own_down), (wout_h, wout), (index_h, index),
         (weight_h, weight), (stream_h, stream), (gain1_h, gain1), (bias1_h, bias1),
         (shared_gate_h, shared_gate), (shared_up_h, shared_up), (shared_down_h, shared_down),
         (gain2_h, gain2), (bias2_h, bias2),
     )
-    loads = [load(k, src, dst) for k, (src, dst) in enumerate(names)]
-
-    barrier = pltpu.get_barrier_semaphore()
-
-    def greet(sp_to, tp_to):
-        pl.semaphore_signal(
-            barrier, inc=1, device_id={"sp": sp_to, "tp": tp_to}, device_id_type=MESH
-        )
-
-    for d in range(1, PLANE):
-        greet(plane_peer(d), tp)
-    for d in range(1, PLANES):
-        greet(z_peer(d), tp)
-    for d in range(1, TPS):
-        greet(sp, (tp + d) % TPS)
-    greet((sp + 63) % 64, tp)
+    loads = []
+    for k, (src, dst) in enumerate(names):
+        loads.append(pltpu.make_async_copy(src, dst, load_sem.at[k]))
+        loads[-1].start()
+    wholes = (gate_up.at[0], gate_up.at[1], down_w)
+    owns = (own_gate, own_up, own_down)
+    slot_loads = [
+        pltpu.make_async_copy(src, dst.at[tp], slot_sem.at[m])
+        for m, (src, dst) in enumerate(zip((gate_w_h, up_w_h, down_w_h), wholes))
+    ]
+
+    @pl.when(owner)
+    def _():
+        for copy in slot_loads:
+            copy.start()
 
     phase("wait_loads")
-    for k in range(6):
+    length = rec.shape[0]
+    loads[0].wait()
+    phase("barrier")
+    pl.semaphore_wait(barrier, 7 + 7 + 3 + 1 + 8)
+    phase("send_gate")
+    border_out = rec.at[length - HEAD_ROWS :]
+    send(border_out, border, border_sem.at[0], border_sem.at[1], (sp + 1) % 64, tp)
+
+    FROM_MATE, FROM_MIRROR, FROM_FAR = range(3)
+    origin = {FROM_MATE: mate, FROM_MIRROR: mirror, FROM_FAR: far}
+    TO_SIBLING, ACROSS = range(2)
+
+    def piece_of(ref, k, lead=()):
+        if k < 4:
+            return ref.at[(*lead, slice(1024 * (k % 2), 1024 * (k % 2) + 1024))]
+        return ref.at[(*lead, slice(None), slice(512 * (k - 4), 512 * (k - 4) + 512))]
+
+    def buffer_of(k):
+        return k // 2 if k < 4 else 2
+
+    def held_piece(k, at):
+        return piece_of(wholes[buffer_of(k)], k, (at,))
+
+    def across(src, k, at, kind, tp_to, when):
+        out = part_out_sem.at[ACROSS, int(k >= 4)]
+        send(src, held_piece(k, at), out, part_sem.at[kind, k], sp, tp_to, when=when)
+
+    def to_sibling(src, k, at):
+        out = part_out_sem.at[TO_SIBLING, int(k >= 4)]
+        lands = guest_sem.at[max(k - 3, 0)]
+        send(src, held_piece(k, at), out, lands, sibling, tp, when=owner)
+
+    def own_out(k):
+        src = piece_of(owns[buffer_of(k)], k)
+        across(src, k, tp, FROM_MATE, mate, owner)
+
+    def own_mirror(k):
+        src = piece_of(owns[buffer_of(k)], k)
+        across(src, k, tp, FROM_MIRROR, mirror, guest)
+
+    def relay(k, kind):
+        got = held_piece(k, origin[kind])
+
+        @pl.when(owner)
+        def _():
+            came(got, part_sem.at[kind, k])
+
+        if kind == FROM_MIRROR:
+            across(got, k, origin[kind], FROM_FAR, mate, owner)
+        to_sibling(got, k, origin[kind])
+
+    for k in (7, 8):
         loads[k].wait()
-    length = rec.shape[0]
+    for k in (0, 1, 2):
+        own_out(k)
+        own_mirror(k)
+
     phase("prepare")
+    for k in range(1, 6):
+        loads[k].wait()
     for g in range(2):
         rec_f[HEAD_ROWS:, 256 * g : 256 * g + 256] = rec[:, g, :].astype(F32)
         extra[:, 256 * g : 256 * g + 256] = extra_raw[:, g, :]
@@ -194,28 +278,11 @@
 
     phase("scan_tail")
     scanned(HEAD_ROWS, length - HEAD_ROWS)
-    phase("barrier")
-
-    pl.semaphore_wait(barrier, 7 + 7 + 3 + 1)
-    send(rec.at[length - HEAD_ROWS :], border, border_sem, (), (sp + 1) % 64, tp)
-
-    left = (tp + 3) % TPS
-    right = (tp + 1) % TPS
-
-    def weights_out(buf, slot, to, k):
-        send(buf.at[slot], buf.at[slot], weight_sem, (k,), sp, to)
-
-    def weights_in(buf, slot, k):
-        remote(buf.at[slot], buf.at[slot], weight_sem, (k,), sp, left).wait_recv()
-
-    opposite = (tp + 2) % TPS
-    phase("send_gate")
-    loads[7].wait()
-    weights_out(gate_w, tp, left, 0)
-    weights_out(gate_w, tp, right, 1)
-
+    loads[9].wait()
+    for k in range(8):
+        to_sibling(piece_of(owns[buffer_of(k)], k), k, tp)
     phase("border")
-    remote(rec.at[length - HEAD_ROWS :], border, border_sem, (), sp, tp).wait_recv()
+    came(border, border_sem.at[1])
     phase("scan_head")
     for g in range(2):
         border_f = border[:, g, :].astype(F32)
@@ -235,7 +302,7 @@
         mine1[0, b : b + 1, :] = total_p[:, 128 * b : 128 * b + 128]
         mine1[1, b : b + 1, :] = total_s[:, 128 * b : 128 * b + 128]
     for d in FAR_FIRST:
-        send(mine1, mine1, carry_sem, (0, d), plane_peer(d), tp)
+        send(mine1, mine1, carry_sem.at[0, 0], carry_sem.at[1, 0], plane_peer(d), tp)
 
     phase("slots")
     for k in (6, 11, 12):
@@ -267,9 +334,7 @@
         gelu_buf[:, 256 * g : 256 * g + 256] = jax.nn.gelu(gatein[:, g, :].astype(F32))
     phase("carry1")
 
-    for d in FAR_FIRST:
-        got = carry1.at[(pi + PLANE - d) % PLANE]
-        remote(got, got, carry_sem, (0, d), sp, tp).wait_recv()
+    came(carry1.at[0:7], carry_sem.at[1, 0])
     one = jnp.ones((4, 128), F32)
     nought = jnp.zeros((4, 128), F32)
     all_p, all_s, in_p, in_s = one, nought, one, nought
@@ -282,11 +347,9 @@
     mine2[0] = all_p
     mine2[1] = all_s
     for d in FAR_FIRST:
-        send(mine2, mine2, carry_sem, (1, d), z_peer(d), tp)
+        send(mine2, mine2, carry_sem.at[0, 1], carry_sem.at[1, 1], z_peer(d), tp)
     phase("carry2")
-    for d in FAR_FIRST:
-        got = carry2.at[(zi + PLANES - d) % PLANES]
-        remote(got, got, carry_sem, (1, d), sp, tp).wait_recv()
+    came(carry2.at[0:7], carry_sem.at[1, 1])
     phase("fixup")
     planes_s = nought
     for k in range(PLANES):
@@ -307,24 +370,21 @@
         part[:, :, cols] = value.reshape(TPS, 32, 512)
         for d in (2, 1, 3):
             to = (tp + d) % TPS
-            send(part.at[to, :, cols], mixed_buf.at[tp, :, cols], mix_sem, (c, d), sp, to)
+            lands = mixed_buf.at[tp, :, cols]
+            send(part.at[to, :, cols], lands, mix_sem.at[0], mix_sem.at[1], sp, to)
     phase("gate_arrive")
-    for k in (8, 9):
-        loads[k].wait()
-    weights_out(up_w, tp, left, 2)
-    weights_out(up_w, tp, right, 3)
-    weights_in(gate_w, right, 0)
-    weights_in(gate_w, left, 1)
-    weights_out(gate_w, right, left, 4)
+    own_out(3)
+    own_mirror(3)
+    for k in (0, 1, 2):
+        relay(k, FROM_MIRROR)
+    for k in (4, 5, 6, 7):
+        own_mirror(k)
+    for k in (0, 1, 2):
+        relay(k, FROM_MATE)
     phase("mix_arrive")
     for k in (13, 14, 15):
         loads[k].wait()
-    for c in range(4):
-        cols = slice(512 * c, 512 * c + 512)
-        for d in (2, 1, 3):
-            came = (tp + TPS - d) % TPS
-            got = mixed_buf.at[came, :, cols]
-            remote(got, got, mix_sem, (c, d), sp, tp).wait_recv()
+    came(mixed_buf.at[0:3], mix_sem.at[1])
     phase("norm1")
     mixed = part[tp].astype(F32)
     for d in (1, 2, 3):
@@ -335,20 +395,71 @@
 
     width = 2048 // CHUNKS
 
-    def exchange(src, dst, sem, hop, c, me, peer):
-        cols = slice(width * c, width * c + width)
-        size = src.shape[0]
+    def cols_of(c):
+        return slice(width * c, width * c + width)
+
+    def z_out(src, dst, trip, c):
+        cols = cols_of(c)
         for d in FAR_FIRST:
-            to = (me + d) % size
-            send(src.at[to, :, cols], dst.at[me, :, cols], sem, (hop, c, d), peer(d), tp)
-        dst[me, :, cols] = src[me, :, cols]
-
-    def arrived(dst, sem, hop, c, me):
-        cols = slice(width * c, width * c + width)
-        size = dst.shape[0]
-        for d in FAR_FIRST:
-            got = dst.at[(me + size - d) % size, :, cols]
-            remote(got, got, sem, (hop, c, d), sp, tp).wait_recv()
+            to = (zi + d) % PLANES
+            lands = dst.at[zi, :, cols]
+            send(
+                src.at[to, :, cols], lands, hop_out_sem.at[trip, 0], z_sem.at[trip, c], z_peer(d), tp
+            )
+        dst[zi, :, cols] = src[zi, :, cols]
+
+    def z_in(dst, trip, c):
+        came(dst.at[0:7, :, cols_of(c)], z_sem.at[trip, c])
+
+    def plane_in(dst, trip, c):
+        @pl.when(owner)
+        def _():
+            came(dst.at[0:7, :, cols_of(c)], p_sem.at[trip, c])
+
+        @pl.when(guest)
+        def _():
+            came(dst.at[:, :, cols_of(c)], p_sem.at[trip, c])
+
+    def plane_out(src, dst, c):
+        cols = cols_of(c)
+        for dx in (2, 1, 3, 0):
+            x_to = (xi + dx) % 4
+            for other in (1, 0):
+                expert = hosted + other * (1 - 2 * hosted)
+                send(
+                    src.at[x_to * 2 + expert, :, cols],
+                    dst.at[pi, :, cols],
+                    hop_out_sem.at[0, 1],
+                    p_sem.at[0, c],
+                    zi * PLANE + x_to * 2 + hosted,
+                    mirror if other else tp,
+                    when=guest if dx == 0 and other == 0 else None,
+                )
+
+        @pl.when(owner)
+        def _():
+            dst[pi, :, cols] = src[pi, :, cols]
+
+    home = jnp.where(owner, tp, mirror)
+
+    def plane_back(src, dst, c):
+        cols = cols_of(c)
+        for dx in (2, 1, 3, 0):
+            for target_core in (0, 1):
+                j = ((xi + dx) % 4) * 2 + target_core
+                send(
+                    src.at[j, :, cols],
+                    dst.at[xi * 2 + hosted, :, cols],
+                    hop_out_sem.at[1, 1],
+                    p_sem.at[1, c],
+                    zi * PLANE + j,
+                    home,
+                    when=jnp.logical_or(guest, core != target_core) if dx == 0 else None,
+                )
+
+        @pl.when(owner)
+        def _():
+            dst[pi, :, cols] = src[pi, :, cols]
 
     def swapped(src, c):
         cols = slice(width * c, width * c + width)
@@ -364,13 +475,7 @@
         cols = slice(width * c, width * c + width)
         value = dot(slot_buf[...], normed[:, cols]).astype(BF16)
         disp[:, :, cols] = value.reshape(8, 16, width)
-        exchange(disp, arr1, disp_sem, 0, c, zi, z_peer)
-    phase("up_from_left")
-    weights_out(down_w, tp, left, 6)
-    weights_in(up_w, left, 3)
-    weights_out(up_w, left, right, 5)
-    weights_out(down_w, tp, right, 7)
-
+        z_out(disp, arr1, 0, c)
     phase("shared")
     for k in (16, 17, 18, 19, 20):
         loads[k].wait()
@@ -378,68 +483,122 @@
     hidden = jax.nn.silu(dot(rows, shared_gate[...])) * dot(rows, shared_up[...])
     acc[...] = RESIDUAL_SCALE * rows.astype(F32) + dot(hidden.astype(BF16), shared_down[...])
 
+    phase("relay_mid")
+    relay(3, FROM_MIRROR)
+    own_out(4)
+    relay(3, FROM_MATE)
+
     for c in range(CHUNKS):
-        cols = slice(width * c, width * c + width)
         phase(f"disp_z_{c}")
-        arrived(arr1, disp_sem, 0, c, zi)
+        z_in(arr1, 0, c)
         phase(f"disp_swap_{c}")
-        disp2[:, :, cols] = swapped(arr1, c)
-        exchange(disp2, arr2, disp_sem, 1, c, pi, plane_peer)
-
+        disp2[:, :, cols_of(c)] = swapped(arr1, c)
+        plane_out(disp2, arr2, c)
+        if c == CHUNKS // 2 - 1:
+            phase("relay_down")
+            for k in (4, 5):
+                relay(k, FROM_MIRROR)
+                own_out(k + 1)
+            relay(0, FROM_FAR)
+
+    phase("far_gate_up")
+    for k in (6, 7):
+        relay(k, FROM_MIRROR)
+        if k == 6:
+            own_out(7)
+    for k in (1, 2, 3):
+        relay(k, FROM_FAR)
+    phase("gate_up_guest")
+
+    @pl.when(owner)
+    def _():
+        for copy in slot_loads:
+            copy.wait()
+
+    @pl.when(guest)
+    def _():
+        came(gate_up, guest_sem.at[0])
+
+    both = None
     for c in range(CHUNKS):
+        cols = cols_of(c)
         phase(f"disp_p_{c}")
-        arrived(arr2, disp_sem, 1, c, pi)
-    phase("gate_opposite")
-    weights_in(up_w, right, 2)
-    picked = arr2[...].reshape(128, 2048)
-    weights_in(gate_w, opposite, 4)
-    phase("gated")
-    gated = [dot(picked, gate_w[k]) for k in range(TPS)]
-    phase("up_opposite")
-    weights_in(up_w, opposite, 5)
-    phase("lifted")
-    lifted = [dot(picked, up_w[k]) for k in range(TPS)]
+        plane_in(arr2, 0, c)
+        phase(f"gate_up_{c}")
+        picked = arr2[:, :, cols].reshape(128, width)
+        terms = [
+            dot(picked, jnp.concatenate([gate_up[0, k, cols], gate_up[1, k, cols]], axis=1))
+            for k in range(TPS)
+        ]
+        both = terms if both is None else [x + y for x, y in zip(both, terms)]
+    phase("hidden")
     hidden = jnp.concatenate(
-        [(jax.nn.silu(g) * u).astype(BF16) for g, u in zip(gated, lifted)], axis=1
+        [(jax.nn.silu(x[:, :128]) * x[:, 128:]).astype(BF16) for x in both], axis=1
     )
-    phase("down_arrive")
-    half = 64
-    weights_in(down_w, right, 6)
-    right_half = down_w.at[right, :half]
-    send(right_half, right_half, weight_sem, (8,), sp, left)
-    weights_in(down_w, left, 7)
-    left_half = down_w.at[left, half:]
-    send(left_half, left_half, weight_sem, (9,), sp, right)
-    phase("down_opposite")
-    low, high = down_w.at[opposite, :half], down_w.at[opposite, half:]
-    remote(low, low, weight_sem, (8,), sp, left).wait_recv()
-    remote(high, high, weight_sem, (9,), sp, left).wait_recv()
+
+    def back_through_plane(c):
+        phase(f"ret_p_{c}")
+        plane_in(ret1, 1, c)
+        phase(f"ret_swap_{c}")
+        ret1p[:, :, cols_of(c)] = swapped(ret1, c)
+        z_out(ret1p, ret2, 1, c)
+
     for c in range(CHUNKS):
-        cols = slice(width * c, width * c + width)
+        cols = cols_of(c)
+        phase(f"down_arrive_{c}")
+        relay(4 + c, FROM_MATE)
+        relay(4 + c, FROM_FAR)
+        phase(f"down_guest_{c}")
+
+        @pl.when(guest)
+        def _():
+            came(down_w.at[:, :, cols], guest_sem.at[1 + c])
+
         phase(f"down_{c}")
         value = dot(hidden, down_w[:, :, cols].reshape(512, width)).astype(BF16)
         moe_out[:, :, cols] = value.reshape(8, 16, width)
-        exchange(moe_out, ret1, ret_sem, 0, c, pi, plane_peer)
-
+        plane_back(moe_out, ret1, c)
+        if c >= 1:
+            back_through_plane(c - 1)
+
+    back_through_plane(CHUNKS - 1)
     for c in range(CHUNKS):
-        cols = slice(width * c, width * c + width)
-        phase(f"ret_p_{c}")
-        arrived(ret1, ret_sem, 0, c, pi)
-        phase(f"ret_swap_{c}")
-        ret1p[:, :, cols] = swapped(ret1, c)
-        exchange(ret1p, ret2, ret_sem, 1, c, zi, z_peer)
-    for c in range(CHUNKS):
-        cols = slice(width * c, width * c + width)
+        cols = cols_of(c)
         phase(f"ret_z_{c}")
-        arrived(ret2, ret_sem, 1, c, zi)
+        z_in(ret2, 1, c)
         phase(f"combine_{c}")
         back = ret2[:, :, cols].reshape(128, width)
         acc[:, cols] = acc[:, cols] + dot(weight_buf[0], back) + dot(weight_buf[1], back)
     phase("norm2")
     out_ref[...] = layer_norm(acc[...], gain2[...], bias2[...]).astype(BF16)
     phase("drain")
-    for copy in sends:
-        copy.wait_send()
+    left(border_out, border_sem.at[0])
+    left(carry1.at[0:7], carry_sem.at[0, 0])
+    left(carry2.at[0:7], carry_sem.at[0, 1])
+    left(part.at[0:3], mix_sem.at[0])
+    for trip, (z_src, p_src) in enumerate(((disp, disp2), (ret1p, moe_out))):
+        left(z_src.at[0:7], hop_out_sem.at[trip, 0])
+
+        @pl.when(owner)
+        def _():
+            left(p_src.at[0:7], hop_out_sem.at[trip, 1])
+
+        @pl.when(guest)
+        def _():
+            left(p_src, hop_out_sem.at[trip, 1])
+
+    @pl.when(owner)
+    def _():
+        left(gate_up, part_out_sem.at[TO_SIBLING, 0])
+        left(down_w, part_out_sem.at[TO_SIBLING, 1])
+        left(gate_up.at[:, 0:2], part_out_sem.at[ACROSS, 0])
+        left(down_w.at[0:2], part_out_sem.at[ACROSS, 1])
+
+    @pl.when(guest)
+    def _():
+        left(gate_up.at[0, 0:2], part_out_sem.at[ACROSS, 0])
+        left(down_w.at[0], part_out_sem.at[ACROSS, 1])
+
     phase()
 
 
@@ -473,11 +632,7 @@
         second_norm_gain.reshape(1, 2048),
         second_norm_bias.reshape(1, 2048),
     )
-    gathered = {13: (4, 2048, 128), 14: (4, 2048, 128), 15: (4, 128, 2048)}
-    held = [
-        pltpu.VMEM(gathered.get(k, operand.shape), operand.dtype)
-        for k, operand in enumerate(operands)
-    ]
+    held = [pltpu.VMEM(operand.shape, operand.dtype) for operand in operands]
     wide = pltpu.VMEM((8, 16, 2048), BF16)
     return pl.pallas_call(
         mega,
@@ -486,6 +641,8 @@
         out_specs=pl.BlockSpec(memory_space=pltpu.VMEM),
         scratch_shapes=[
             *held,
+            pltpu.VMEM((2, TPS, 2048, 128), BF16),
+            pltpu.VMEM((TPS, 128, 2048), BF16),
             pltpu.VMEM((128, 512), F32),
             pltpu.VMEM((2, 128, 8), F32),
             pltpu.VMEM((128 + HEAD_ROWS, 512), F32),
@@ -504,13 +661,16 @@
             wide, wide, wide, wide, wide, wide, wide, wide,
             pltpu.VMEM((32, 2048), F32),
             pltpu.SemaphoreType.DMA((len(operands),)),
+            pltpu.SemaphoreType.DMA((3,)),
             pltpu.SemaphoreType.DMA((2,)),
+            pltpu.SemaphoreType.DMA((3, 8)),
+            pltpu.SemaphoreType.DMA((5,)),
+            pltpu.SemaphoreType.DMA((2, 2)),
+            pltpu.SemaphoreType.DMA((2, 2)),
             pltpu.SemaphoreType.DMA((2,)),
-            pltpu.SemaphoreType.DMA((2, 10)),
-            pltpu.SemaphoreType.DMA((2, 2, 8)),
-            pltpu.SemaphoreType.DMA((2, 4, 4)),
-            pltpu.SemaphoreType.DMA((2, 2, CHUNKS, 8)),
-            pltpu.SemaphoreType.DMA((2, 2, CHUNKS, 8)),
+            pltpu.SemaphoreType.DMA((2, CHUNKS)),
+            pltpu.SemaphoreType.DMA((2, CHUNKS)),
+            pltpu.SemaphoreType.DMA((2, 2)),
         ],
         compiler_params=pltpu.CompilerParams(
             collective_id=0, has_side_effects=True, vmem_limit_bytes=56 * 2**20

time: 93.8 us -> 70.7 us (0.75)
  Pallas kernels: 92.1 us -> 68.8 us
    pallas_call x1, Pallas kernels: 92.1 us -> 68.8 us  [shards(): pl.pallas_call(mega, out_shape=jax.ShapeDtypeStruct((32, 2048), BF16), in...]
where the time goes in v4:
time: 70.7 us; the launch traced here: 70.4 us
  Pallas kernels  68.8 us (97%)
  local copies, waits for them, and re-layouts  1.57 us (2%)
    pallas_call x1, Pallas kernels, shards(): pl.pallas_call(mega, out_shape=jax.ShapeDtypeStruct((32, 2048), BF16), in...  68.8 us
    unnamed x1, local copies, waits for them, and re-layouts  1.57 us

profile of v4, /device:TPU:1, one launch (start us, length us, event | category | flops | bytes accessed | tf_op | source)
XLA Modules:
  0.0 70.4 jit_solution(15648120649743767078)
XLA Ops:
  0.0 68.8 %mega.1 = bf16[32,2048]{1,0:T(8,128)(2,1)} custom-call(bf16[32,2048]{1,0:T(8,128)(2,1)} %stream_h.1, bf16[128,2,256]{2,1,0:T(2,128)(2,1)} %rec_h.1, bf16[128,2,256]{2,1,0:T(2,128)(2,1)} %gatein_h.1, bf16[4,2,256]{2,1,0:T(2,128)(2,1)} %taps_h.1, bf16[2,4,64,64]{3,2,1,0:T(8,128)(2,1)} %small_gates_h.1, bf16[2,2,128,128]{3,2,1,0:T(8,128)(2,1)} %large_gates_h.1, ...), custom_call_target="tpu_custom_call" | custom-call | tf_op jit(solution)/shard_map/mega/pallas_call | solution.py:637
  68.9 1.6 %copy.23 = bf16[32,2048]{1,0:T(8,128)(2,1)} copy(bf16[32,2048]{1,0:T(8,128)(2,1)} %mega.1) | data formatting | bytes 262144

commit v5 on v4

--- a/solution.py
+++ b/solution.py
@@ -72,7 +72,7 @@
     extra, turned, rec_f, border, cum_p, cum_s, carry1, carry2, gelu_buf, branch,
     part, mixed_buf, normed, slot_buf, weight_buf,
     disp, arr1, disp2, arr2, moe_out, ret1, ret1p, ret2, acc,
-    load_sem, slot_sem, border_sem, part_sem, guest_sem, part_out_sem, carry_sem, mix_sem,
+    load_sem, slot_sem, border_sem, part_sem, guest_sem, part_out_sem, carry_sem, plane_sem, mix_sem,
     z_sem, p_sem, hop_out_sem,
 ):
     sp = lax.axis_index("sp")
@@ -215,7 +215,7 @@
 
     for k in (7, 8):
         loads[k].wait()
-    for k in (0, 1, 2):
+    for k in (0, 1, 2, 3):
         own_out(k)
         own_mirror(k)
 
@@ -302,7 +302,7 @@
         mine1[0, b : b + 1, :] = total_p[:, 128 * b : 128 * b + 128]
         mine1[1, b : b + 1, :] = total_s[:, 128 * b : 128 * b + 128]
     for d in FAR_FIRST:
-        send(mine1, mine1, carry_sem.at[0, 0], carry_sem.at[1, 0], plane_peer(d), tp)
+        send(mine1, mine1, carry_sem.at[0], carry_sem.at[1], plane_peer(d), tp)
 
     phase("slots")
     for k in (6, 11, 12):
@@ -325,16 +325,24 @@
     )
     earlier = dot(below.astype(BF16), named.astype(BF16))
     right_slot = jnp.abs(earlier - (slot % 2).astype(F32)) < 0.5
-    slot_buf[...] = jnp.where(right_slot, named, 0.0).T.astype(BF16)
+    to_row = lax.broadcasted_iota(jnp.int32, (128, 128), 0)
+    from_row = lax.broadcasted_iota(jnp.int32, (128, 128), 1)
+    outer, inner, pair = to_row // 16, (to_row // 2) % 8, to_row % 2
+    pick = (from_row == inner * 16 + outer * 2 + pair).astype(BF16)
+    slot_rows = jnp.where(right_slot, named, 0.0).T.astype(BF16)
+    slot_buf[0] = slot_rows
+    slot_buf[1] = dot(pick, slot_rows).astype(BF16)
     scaled = jnp.where(right_slot, scaled, 0.0)
     high = scaled.astype(BF16)
-    weight_buf[0] = high
-    weight_buf[1] = (scaled - high.astype(F32)).astype(BF16)
+    low = (scaled - high.astype(F32)).astype(BF16)
+    for part_no, values in enumerate((high, low)):
+        weight_buf[part_no] = dot(values, pick).astype(BF16)
+        weight_buf[2 + part_no] = values
     for g in range(2):
         gelu_buf[:, 256 * g : 256 * g + 256] = jax.nn.gelu(gatein[:, g, :].astype(F32))
     phase("carry1")
 
-    came(carry1.at[0:7], carry_sem.at[1, 0])
+    came(carry1.at[0:7], carry_sem.at[1])
     one = jnp.ones((4, 128), F32)
     nought = jnp.zeros((4, 128), F32)
     all_p, all_s, in_p, in_s = one, nought, one, nought
@@ -346,10 +354,24 @@
     mine2 = carry2.at[zi]
     mine2[0] = all_p
     mine2[1] = all_s
-    for d in FAR_FIRST:
-        send(mine2, mine2, carry_sem.at[0, 1], carry_sem.at[1, 1], z_peer(d), tp)
+    for d in (4, 3, 5, 2, 6, 1, 7):
+        send(
+            mine2,
+            mine2,
+            plane_sem.at[0, d - 1],
+            plane_sem.at[1, d - 1],
+            z_peer(d),
+            tp,
+            when=zi + d < PLANES,
+        )
     phase("carry2")
-    came(carry2.at[0:7], carry_sem.at[1, 1])
+    for d in range(1, PLANES):
+        got = carry2.at[(zi + PLANES - d) % PLANES]
+
+        @pl.when(zi >= d)
+        def _():
+            came(got, plane_sem.at[1, d - 1])
+
     phase("fixup")
     planes_s = nought
     for k in range(PLANES):
@@ -373,13 +395,12 @@
             lands = mixed_buf.at[tp, :, cols]
             send(part.at[to, :, cols], lands, mix_sem.at[0], mix_sem.at[1], sp, to)
     phase("gate_arrive")
-    own_out(3)
-    own_mirror(3)
-    for k in (0, 1, 2):
-        relay(k, FROM_MIRROR)
     for k in (4, 5, 6, 7):
         own_mirror(k)
-    for k in (0, 1, 2):
+    for k in (0, 1, 2, 3):
+        relay(k, FROM_MIRROR)
+    own_out(4)
+    for k in (0, 1, 2, 3):
         relay(k, FROM_MATE)
     phase("mix_arrive")
     for k in (13, 14, 15):
@@ -462,20 +483,20 @@
             dst[pi, :, cols] = src[pi, :, cols]
 
     def swapped(src, c):
-        cols = slice(width * c, width * c + width)
-        to_row = lax.broadcasted_iota(jnp.int32, (128, 128), 0)
-        from_row = lax.broadcasted_iota(jnp.int32, (128, 128), 1)
-        outer, inner, pair = to_row // 16, (to_row // 2) % 8, to_row % 2
-        pick = (from_row == inner * 16 + outer * 2 + pair).astype(BF16)
-        rows = src[:, :, cols].reshape(128, width)
+        rows = src[:, :, cols_of(c)].reshape(128, width)
         return dot(pick, rows).astype(BF16).reshape(8, 16, width)
 
-    phase("dispatch")
-    for c in range(CHUNKS):
-        cols = slice(width * c, width * c + width)
-        value = dot(slot_buf[...], normed[:, cols]).astype(BF16)
+    Z_FIRST = tuple(range(CHUNKS // 2))
+    P_FIRST = tuple(range(CHUNKS // 2, CHUNKS))
+    for c in (*Z_FIRST, *P_FIRST):
+        cols = cols_of(c)
+        order = int(c in P_FIRST)
+        value = dot(slot_buf[order], normed[:, cols]).astype(BF16)
         disp[:, :, cols] = value.reshape(8, 16, width)
-        z_out(disp, arr1, 0, c)
+        if c in Z_FIRST:
+            z_out(disp, arr1, 0, c)
+        else:
+            plane_out(disp, arr1, c)
     phase("shared")
     for k in (16, 17, 18, 19, 20):
         loads[k].wait()
@@ -484,28 +505,29 @@
     acc[...] = RESIDUAL_SCALE * rows.astype(F32) + dot(hidden.astype(BF16), shared_down[...])
 
     phase("relay_mid")
-    relay(3, FROM_MIRROR)
-    own_out(4)
-    relay(3, FROM_MATE)
-
-    for c in range(CHUNKS):
-        phase(f"disp_z_{c}")
+    relay(4, FROM_MIRROR)
+    own_out(5)
+
+    for c in P_FIRST:
+        phase(f"disp_p1_{c}")
+        plane_in(arr1, 0, c)
+        phase(f"disp_swap_{c}")
+        disp2[:, :, cols_of(c)] = swapped(arr1, c)
+        z_out(disp2, arr2, 0, c)
+    phase("relay_down")
+    for k in (5, 6, 7):
+        relay(k, FROM_MIRROR)
+        if k < 7:
+            own_out(k + 1)
+    relay(0, FROM_FAR)
+    for c in Z_FIRST:
+        phase(f"disp_z1_{c}")
         z_in(arr1, 0, c)
         phase(f"disp_swap_{c}")
         disp2[:, :, cols_of(c)] = swapped(arr1, c)
         plane_out(disp2, arr2, c)
-        if c == CHUNKS // 2 - 1:
-            phase("relay_down")
-            for k in (4, 5):
-                relay(k, FROM_MIRROR)
-                own_out(k + 1)
-            relay(0, FROM_FAR)
 
     phase("far_gate_up")
-    for k in (6, 7):
-        relay(k, FROM_MIRROR)
-        if k == 6:
-            own_out(7)
     for k in (1, 2, 3):
         relay(k, FROM_FAR)
     phase("gate_up_guest")
@@ -520,12 +542,21 @@
         came(gate_up, guest_sem.at[0])
 
     both = None
-    for c in range(CHUNKS):
+    for n, c in enumerate([c for both_kinds in zip(Z_FIRST, P_FIRST) for c in both_kinds]):
         cols = cols_of(c)
-        phase(f"disp_p_{c}")
-        plane_in(arr2, 0, c)
-        phase(f"gate_up_{c}")
-        picked = arr2[:, :, cols].reshape(128, width)
+        if n == CHUNKS - 1:
+            phase("relay_down_0")
+            relay(4, FROM_MATE)
+            relay(4, FROM_FAR)
+        phase(f"disp_2_{c}")
+        if c in Z_FIRST:
+            plane_in(arr2, 0, c)
+            phase(f"gate_up_{c}")
+            picked = arr2[:, :, cols].reshape(128, width)
+        else:
+            z_in(arr2, 0, c)
+            phase(f"gate_up_{c}")
+            picked = swapped(arr2, c).reshape(128, width)
         terms = [
             dot(picked, jnp.concatenate([gate_up[0, k, cols], gate_up[1, k, cols]], axis=1))
             for k in range(TPS)
@@ -536,18 +567,27 @@
         [(jax.nn.silu(x[:, :128]) * x[:, 128:]).astype(BF16) for x in both], axis=1
     )
 
-    def back_through_plane(c):
-        phase(f"ret_p_{c}")
-        plane_in(ret1, 1, c)
+    hidden_by_z = dot(pick, hidden).astype(BF16)
+
+    def second_hop(c):
+        phase(f"ret_1_{c}")
+        if c in Z_FIRST:
+            z_in(ret1, 1, c)
+        else:
+            plane_in(ret1, 1, c)
         phase(f"ret_swap_{c}")
         ret1p[:, :, cols_of(c)] = swapped(ret1, c)
-        z_out(ret1p, ret2, 1, c)
+        if c in Z_FIRST:
+            plane_back(ret1p, ret2, c)
+        else:
+            z_out(ret1p, ret2, 1, c)
 
     for c in range(CHUNKS):
         cols = cols_of(c)
         phase(f"down_arrive_{c}")
-        relay(4 + c, FROM_MATE)
-        relay(4 + c, FROM_FAR)
+        if c > 0:
+            relay(4 + c, FROM_MATE)
+            relay(4 + c, FROM_FAR)
         phase(f"down_guest_{c}")
 
         @pl.when(guest)
@@ -555,26 +595,42 @@
             came(down_w.at[:, :, cols], guest_sem.at[1 + c])
 
         phase(f"down_{c}")
-        value = dot(hidden, down_w[:, :, cols].reshape(512, width)).astype(BF16)
+        rows = hidden_by_z if c in Z_FIRST else hidden
+        value = dot(rows, down_w[:, :, cols].reshape(512, width)).astype(BF16)
         moe_out[:, :, cols] = value.reshape(8, 16, width)
-        plane_back(moe_out, ret1, c)
-        if c >= 1:
-            back_through_plane(c - 1)
-
-    back_through_plane(CHUNKS - 1)
+        if c in Z_FIRST:
+            z_out(moe_out, ret1, 1, c)
+        else:
+            plane_back(moe_out, ret1, c)
+        if c == CHUNKS - 2:
+            second_hop(0)
+
+    for c in range(1, CHUNKS):
+        second_hop(c)
     for c in range(CHUNKS):
         cols = cols_of(c)
-        phase(f"ret_z_{c}")
-        z_in(ret2, 1, c)
+        phase(f"ret_2_{c}")
+        if c in Z_FIRST:
+            plane_in(ret2, 1, c)
+        else:
+            z_in(ret2, 1, c)
         phase(f"combine_{c}")
         back = ret2[:, :, cols].reshape(128, width)
-        acc[:, cols] = acc[:, cols] + dot(weight_buf[0], back) + dot(weight_buf[1], back)
+        order = 0 if c in Z_FIRST else 2
+        acc[:, cols] = (
+            acc[:, cols] + dot(weight_buf[order], back) + dot(weight_buf[order + 1], back)
+        )
     phase("norm2")
     out_ref[...] = layer_norm(acc[...], gain2[...], bias2[...]).astype(BF16)
     phase("drain")
     left(border_out, border_sem.at[0])
-    left(carry1.at[0:7], carry_sem.at[0, 0])
-    left(carry2.at[0:7], carry_sem.at[0, 1])
+    left(carry1.at[0:7], carry_sem.at[0])
+    for d in range(1, PLANES):
+
+        @pl.when(zi + d < PLANES)
+        def _():
+            left(mine2, plane_sem.at[0, d - 1])
+
     left(part.at[0:3], mix_sem.at[0])
     for trip, (z_src, p_src) in enumerate(((disp, disp2), (ret1p, moe_out))):
         left(z_src.at[0:7], hop_out_sem.at[trip, 0])
@@ -656,8 +712,8 @@
             pltpu.VMEM((TPS, 32, 2048), BF16),
             pltpu.VMEM((TPS, 32, 2048), BF16),
             pltpu.VMEM((32, 2048), BF16),
-            pltpu.VMEM((128, 32), BF16),
-            pltpu.VMEM((2, 32, 128), BF16),
+            pltpu.VMEM((2, 128, 32), BF16),
+            pltpu.VMEM((4, 32, 128), BF16),
             wide, wide, wide, wide, wide, wide, wide, wide,
             pltpu.VMEM((32, 2048), F32),
             pltpu.SemaphoreType.DMA((len(operands),)),
@@ -666,7 +722,8 @@
             pltpu.SemaphoreType.DMA((3, 8)),
             pltpu.SemaphoreType.DMA((5,)),
             pltpu.SemaphoreType.DMA((2, 2)),
-            pltpu.SemaphoreType.DMA((2, 2)),
+            pltpu.SemaphoreType.DMA((2,)),
+            pltpu.SemaphoreType.DMA((2, 7)),
             pltpu.SemaphoreType.DMA((2,)),
             pltpu.SemaphoreType.DMA((2, CHUNKS)),
             pltpu.SemaphoreType.DMA((2, CHUNKS)),

time: 70.7 us -> 68 us (0.962)
  Pallas kernels: 68.8 us -> 66.3 us
    pallas_call x1, Pallas kernels: 68.8 us -> 66.3 us  [shards(): pl.pallas_call(mega, out_shape=jax.ShapeDtypeStruct((32, 2048), BF16), in...]
where the time goes in v5:
time: 68 us; the launch traced here: 67.9 us
  Pallas kernels  66.3 us (98%)
  local copies, waits for them, and re-layouts  1.57 us (2%)
    pallas_call x1, Pallas kernels, shards(): pl.pallas_call(mega, out_shape=jax.ShapeDtypeStruct((32, 2048), BF16), in...  66.3 us
    unnamed x1, local copies, waits for them, and re-layouts  1.57 us

profile of v5, /device:TPU:1, one launch (start us, length us, event | category | flops | bytes accessed | tf_op | source)
XLA Modules:
  0.0 67.9 jit_solution(6369534056449481340)
XLA Ops:
  0.0 66.3 %mega.1 = bf16[32,2048]{1,0:T(8,128)(2,1)} custom-call(bf16[32,2048]{1,0:T(8,128)(2,1)} %stream_h.1, bf16[128,2,256]{2,1,0:T(2,128)(2,1)} %rec_h.1, bf16[128,2,256]{2,1,0:T(2,128)(2,1)} %gatein_h.1, bf16[4,2,256]{2,1,0:T(2,128)(2,1)} %taps_h.1, bf16[2,4,64,64]{3,2,1,0:T(8,128)(2,1)} %small_gates_h.1, bf16[2,2,128,128]{3,2,1,0:T(8,128)(2,1)} %large_gates_h.1, ...), custom_call_target="tpu_custom_call" | custom-call | tf_op jit(solution)/shard_map/mega/pallas_call | solution.py:693
  66.3 1.6 %copy.23 = bf16[32,2048]{1,0:T(8,128)(2,1)} copy(bf16[32,2048]{1,0:T(8,128)(2,1)} %mega.1) | data formatting | bytes 262144

commit v6 on v5

--- a/solution.py
+++ b/solution.py
@@ -72,8 +72,8 @@
     extra, turned, rec_f, border, cum_p, cum_s, carry1, carry2, gelu_buf, branch,
     part, mixed_buf, normed, slot_buf, weight_buf,
     disp, arr1, disp2, arr2, moe_out, ret1, ret1p, ret2, acc,
-    load_sem, slot_sem, border_sem, part_sem, guest_sem, part_out_sem, carry_sem, plane_sem, mix_sem,
-    z_sem, p_sem, hop_out_sem,
+    load_sem, slot_sem, border_sem, part_sem, part_out_sem, carry_sem, plane_sem, mix_sem,
+    z_sem, p_sem, last_sem, out_sem,
 ):
     sp = lax.axis_index("sp")
     tp = lax.axis_index("tp")
@@ -85,7 +85,7 @@
     mirror = 3 - tp
     mate = tp + 1 - 2 * (tp % 2)
     far = 3 - mate
-    sibling = sp + 1 - 2 * core
+    place = xi * 2 + hosted
     owner = core == hosted
     guest = core != hosted
     phase = Phases()
@@ -136,6 +136,8 @@
     greet((sp + 63) % 64, tp)
     for j in range(PLANE):
         greet(zi * PLANE + j, mirror)
+    for d in FAR_FIRST:
+        greet(z_peer(d) + 1 - 2 * core, tp)
 
     names = (
         (rec_h, rec), (small_gates_h, small_gates), (large_gates_h, large_gates), (taps_h, taps),
@@ -165,14 +167,13 @@
     length = rec.shape[0]
     loads[0].wait()
     phase("barrier")
-    pl.semaphore_wait(barrier, 7 + 7 + 3 + 1 + 8)
+    pl.semaphore_wait(barrier, 7 + 7 + 3 + 1 + 8 + 7)
     phase("send_gate")
     border_out = rec.at[length - HEAD_ROWS :]
     send(border_out, border, border_sem.at[0], border_sem.at[1], (sp + 1) % 64, tp)
 
     FROM_MATE, FROM_MIRROR, FROM_FAR = range(3)
     origin = {FROM_MATE: mate, FROM_MIRROR: mirror, FROM_FAR: far}
-    TO_SIBLING, ACROSS = range(2)
 
     def piece_of(ref, k, lead=()):
         if k < 4:
@@ -186,13 +187,8 @@
         return piece_of(wholes[buffer_of(k)], k, (at,))
 
     def across(src, k, at, kind, tp_to, when):
-        out = part_out_sem.at[ACROSS, int(k >= 4)]
+        out = part_out_sem.at[int(k >= 4)]
         send(src, held_piece(k, at), out, part_sem.at[kind, k], sp, tp_to, when=when)
-
-    def to_sibling(src, k, at):
-        out = part_out_sem.at[TO_SIBLING, int(k >= 4)]
-        lands = guest_sem.at[max(k - 3, 0)]
-        send(src, held_piece(k, at), out, lands, sibling, tp, when=owner)
 
     def own_out(k):
         src = piece_of(owns[buffer_of(k)], k)
@@ -202,16 +198,15 @@
         src = piece_of(owns[buffer_of(k)], k)
         across(src, k, tp, FROM_MIRROR, mirror, guest)
 
-    def relay(k, kind):
-        got = held_piece(k, origin[kind])
-
+    def held(k, kind):
+        came(held_piece(k, origin[kind]), part_sem.at[kind, k])
+
+    def relay(k):
         @pl.when(owner)
         def _():
-            came(got, part_sem.at[kind, k])
-
-        if kind == FROM_MIRROR:
-            across(got, k, origin[kind], FROM_FAR, mate, owner)
-        to_sibling(got, k, origin[kind])
+            held(k, FROM_MIRROR)
+
+        across(held_piece(k, mirror), k, mirror, FROM_FAR, mate, owner)
 
     for k in (7, 8):
         loads[k].wait()
@@ -279,8 +274,6 @@
     phase("scan_tail")
     scanned(HEAD_ROWS, length - HEAD_ROWS)
     loads[9].wait()
-    for k in range(8):
-        to_sibling(piece_of(owns[buffer_of(k)], k), k, tp)
     phase("border")
     came(border, border_sem.at[1])
     phase("scan_head")
@@ -395,13 +388,9 @@
             lands = mixed_buf.at[tp, :, cols]
             send(part.at[to, :, cols], lands, mix_sem.at[0], mix_sem.at[1], sp, to)
     phase("gate_arrive")
-    for k in (4, 5, 6, 7):
-        own_mirror(k)
     for k in (0, 1, 2, 3):
-        relay(k, FROM_MIRROR)
+        relay(k)
     own_out(4)
-    for k in (0, 1, 2, 3):
-        relay(k, FROM_MATE)
     phase("mix_arrive")
     for k in (13, 14, 15):
         loads[k].wait()
@@ -419,47 +408,104 @@
     def cols_of(c):
         return slice(width * c, width * c + width)
 
-    def z_out(src, dst, trip, c):
+    def z_out(src, dst, trip, c, out):
         cols = cols_of(c)
         for d in FAR_FIRST:
             to = (zi + d) % PLANES
             lands = dst.at[zi, :, cols]
-            send(
-                src.at[to, :, cols], lands, hop_out_sem.at[trip, 0], z_sem.at[trip, c], z_peer(d), tp
-            )
+            send(src.at[to, :, cols], lands, out_sem.at[out], z_sem.at[trip, c], z_peer(d), tp)
         dst[zi, :, cols] = src[zi, :, cols]
 
-    def z_in(dst, trip, c):
-        came(dst.at[0:7, :, cols_of(c)], z_sem.at[trip, c])
-
-    def plane_in(dst, trip, c):
+    def by_role(ref_of, sem):
         @pl.when(owner)
         def _():
-            came(dst.at[0:7, :, cols_of(c)], p_sem.at[trip, c])
+            came(ref_of(slice(0, 7)), sem)
 
         @pl.when(guest)
         def _():
-            came(dst.at[:, :, cols_of(c)], p_sem.at[trip, c])
-
-    def plane_out(src, dst, c):
+            came(ref_of(slice(0, 8)), sem)
+
+    def plane_out(src, c, first):
         cols = cols_of(c)
         for dx in (2, 1, 3, 0):
             x_to = (xi + dx) % 4
             for other in (1, 0):
                 expert = hosted + other * (1 - 2 * hosted)
+                if first:
+                    core_to, lands = hosted, arr1.at[pi, :, cols]
+                    recv = p_sem.at[0, c]
+                else:
+                    core_to, lands = expert, arr2.at[other, pi, :, cols]
+                    recv = last_sem.at[other, c]
                 send(
                     src.at[x_to * 2 + expert, :, cols],
-                    dst.at[pi, :, cols],
-                    hop_out_sem.at[0, 1],
-                    p_sem.at[0, c],
-                    zi * PLANE + x_to * 2 + hosted,
+                    lands,
+                    out_sem.at[1 if first else 2],
+                    recv,
+                    zi * PLANE + x_to * 2 + core_to,
                     mirror if other else tp,
                     when=guest if dx == 0 and other == 0 else None,
                 )
 
         @pl.when(owner)
         def _():
-            dst[pi, :, cols] = src[pi, :, cols]
+            if first:
+                arr1[pi, :, cols] = src[pi, :, cols]
+            else:
+                arr2[0, pi, :, cols] = src[pi, :, cols]
+
+    def z_to_expert(src, c):
+        cols = cols_of(c)
+        group = jnp.where(owner, 0, 1)
+        for d in (*FAR_FIRST, 0):
+            to = (zi + d) % PLANES
+            send(
+                src.at[to, :, cols],
+                arr2.at[group, zi, :, cols],
+                out_sem.at[3],
+                last_sem.at[group, c],
+                to * PLANE + place,
+                tp,
+                when=guest if d == 0 else None,
+            )
+
+        @pl.when(owner)
+        def _():
+            arr2[0, zi, :, cols] = src[zi, :, cols]
+
+    def expert_to_z(c):
+        cols = cols_of(c)
+        for d in (*FAR_FIRST, 0):
+            to = (zi + d) % PLANES
+            for group in (0, 1):
+                if d == 0 and group == 0:
+                    ret1[zi, :, cols] = moe_out[0, zi, :, cols]
+                    continue
+                remote(
+                    moe_out.at[group, to, :, cols],
+                    ret1.at[zi, :, cols],
+                    out_sem.at[4 + group],
+                    z_sem.at[1, c],
+                    to * PLANE + place + group * (1 - 2 * hosted),
+                    tp,
+                ).start()
+
+    def expert_to_plane(c):
+        cols = cols_of(c)
+        for d in (*FAR_FIRST, 0):
+            j = (pi + d) % PLANE
+            for group in (1, 0):
+                if d == 0 and group == 0:
+                    ret1[pi, :, cols] = moe_out[0, pi, :, cols]
+                    continue
+                remote(
+                    moe_out.at[group, j, :, cols],
+                    ret1.at[place, :, cols],
+                    out_sem.at[6 + group],
+                    p_sem.at[1, c],
+                    zi * PLANE + j,
+                    mirror if group else tp,
+                ).start()
 
     home = jnp.where(owner, tp, mirror)
 
@@ -470,8 +516,8 @@
                 j = ((xi + dx) % 4) * 2 + target_core
                 send(
                     src.at[j, :, cols],
-                    dst.at[xi * 2 + hosted, :, cols],
-                    hop_out_sem.at[1, 1],
+                    dst.at[place, :, cols],
+                    out_sem.at[8],
                     p_sem.at[1, c],
                     zi * PLANE + j,
                     home,
@@ -481,6 +527,9 @@
         @pl.when(owner)
         def _():
             dst[pi, :, cols] = src[pi, :, cols]
+
+    def permuted(rows):
+        return dot(pick, rows).astype(BF16)
 
     def swapped(src, c):
         rows = src[:, :, cols_of(c)].reshape(128, width)
@@ -494,9 +543,11 @@
         value = dot(slot_buf[order], normed[:, cols]).astype(BF16)
         disp[:, :, cols] = value.reshape(8, 16, width)
         if c in Z_FIRST:
-            z_out(disp, arr1, 0, c)
+            z_out(disp, arr1, 0, c, 0)
         else:
-            plane_out(disp, arr1, c)
+            plane_out(disp, c, True)
+    for k in (4, 5, 6, 7):
+        own_mirror(k)
     phase("shared")
     for k in (16, 17, 18, 19, 20):
         loads[k].wait()
@@ -504,116 +555,87 @@
     hidden = jax.nn.silu(dot(rows, shared_gate[...])) * dot(rows, shared_up[...])
     acc[...] = RESIDUAL_SCALE * rows.astype(F32) + dot(hidden.astype(BF16), shared_down[...])
 
-    phase("relay_mid")
-    relay(4, FROM_MIRROR)
-    own_out(5)
-
     for c in P_FIRST:
         phase(f"disp_p1_{c}")
-        plane_in(arr1, 0, c)
+        by_role(lambda blocks: arr1.at[blocks, :, cols_of(c)], p_sem.at[0, c])
         phase(f"disp_swap_{c}")
         disp2[:, :, cols_of(c)] = swapped(arr1, c)
-        z_out(disp2, arr2, 0, c)
-    phase("relay_down")
-    for k in (5, 6, 7):
-        relay(k, FROM_MIRROR)
-        if k < 7:
-            own_out(k + 1)
-    relay(0, FROM_FAR)
+        z_to_expert(disp2, c)
     for c in Z_FIRST:
         phase(f"disp_z1_{c}")
-        z_in(arr1, 0, c)
+        came(arr1.at[0:7, :, cols_of(c)], z_sem.at[0, c])
         phase(f"disp_swap_{c}")
         disp2[:, :, cols_of(c)] = swapped(arr1, c)
-        plane_out(disp2, arr2, c)
-
-    phase("far_gate_up")
-    for k in (1, 2, 3):
-        relay(k, FROM_FAR)
-    phase("gate_up_guest")
+        plane_out(disp2, c, False)
+        phase(f"relay_{c}")
+        for k in range(4 + 2 * c, 6 + 2 * c):
+            relay(k)
+            if k < 7:
+                own_out(k + 1)
+    phase()
 
     @pl.when(owner)
     def _():
+        phase("weights")
         for copy in slot_loads:
             copy.wait()
-
-    @pl.when(guest)
-    def _():
-        came(gate_up, guest_sem.at[0])
-
-    both = None
-    for n, c in enumerate([c for both_kinds in zip(Z_FIRST, P_FIRST) for c in both_kinds]):
-        cols = cols_of(c)
-        if n == CHUNKS - 1:
-            phase("relay_down_0")
-            relay(4, FROM_MATE)
-            relay(4, FROM_FAR)
-        phase(f"disp_2_{c}")
-        if c in Z_FIRST:
-            plane_in(arr2, 0, c)
+        for kind in (FROM_MATE, FROM_FAR):
+            for k in (0, 1, 2, 3):
+                held(k, kind)
+        both = None
+        for c in [c for both_kinds in zip(Z_FIRST, P_FIRST) for c in both_kinds]:
+            cols = cols_of(c)
+            phase(f"disp_2_{c}")
+            came(arr2.at[0, 0:7, :, cols], last_sem.at[0, c])
+            came(arr2.at[1, :, :, cols], last_sem.at[1, c])
             phase(f"gate_up_{c}")
-            picked = arr2[:, :, cols].reshape(128, width)
-        else:
-            z_in(arr2, 0, c)
-            phase(f"gate_up_{c}")
-            picked = swapped(arr2, c).reshape(128, width)
-        terms = [
-            dot(picked, jnp.concatenate([gate_up[0, k, cols], gate_up[1, k, cols]], axis=1))
-            for k in range(TPS)
-        ]
-        both = terms if both is None else [x + y for x, y in zip(both, terms)]
-    phase("hidden")
-    hidden = jnp.concatenate(
-        [(jax.nn.silu(x[:, :128]) * x[:, 128:]).astype(BF16) for x in both], axis=1
-    )
-
-    hidden_by_z = dot(pick, hidden).astype(BF16)
-
-    def second_hop(c):
+            groups = [arr2[g, :, :, cols].reshape(128, width) for g in (0, 1)]
+            if c in P_FIRST:
+                groups = [permuted(rows) for rows in groups]
+            picked = jnp.concatenate(groups, axis=0)
+            terms = [
+                dot(picked, jnp.concatenate([gate_up[0, k, cols], gate_up[1, k, cols]], axis=1))
+                for k in range(TPS)
+            ]
+            both = terms if both is None else [x + y for x, y in zip(both, terms)]
+        phase("hidden")
+        hidden = jnp.concatenate(
+            [(jax.nn.silu(x[:, :128]) * x[:, 128:]).astype(BF16) for x in both], axis=1
+        )
+        by_plane = hidden
+        by_z = jnp.concatenate([permuted(hidden[:128]), permuted(hidden[128:])], axis=0)
+        for c in range(CHUNKS):
+            cols = cols_of(c)
+            phase(f"down_arrive_{c}")
+            held(4 + c, FROM_MATE)
+            held(4 + c, FROM_FAR)
+            phase(f"down_{c}")
+            rows = by_z if c in Z_FIRST else by_plane
+            value = dot(rows, down_w[:, :, cols].reshape(512, width)).astype(BF16)
+            moe_out[:, :, :, cols] = value.reshape(2, 8, 16, width)
+            if c in Z_FIRST:
+                expert_to_z(c)
+            else:
+                expert_to_plane(c)
+        phase()
+
+    for c in range(CHUNKS):
         phase(f"ret_1_{c}")
-        if c in Z_FIRST:
-            z_in(ret1, 1, c)
-        else:
-            plane_in(ret1, 1, c)
+        sem = z_sem.at[1, c] if c in Z_FIRST else p_sem.at[1, c]
+        by_role(lambda blocks: ret1.at[blocks, :, cols_of(c)], sem)
         phase(f"ret_swap_{c}")
         ret1p[:, :, cols_of(c)] = swapped(ret1, c)
         if c in Z_FIRST:
             plane_back(ret1p, ret2, c)
         else:
-            z_out(ret1p, ret2, 1, c)
-
-    for c in range(CHUNKS):
-        cols = cols_of(c)
-        phase(f"down_arrive_{c}")
-        if c > 0:
-            relay(4 + c, FROM_MATE)
-            relay(4 + c, FROM_FAR)
-        phase(f"down_guest_{c}")
-
-        @pl.when(guest)
-        def _():
-            came(down_w.at[:, :, cols], guest_sem.at[1 + c])
-
-        phase(f"down_{c}")
-        rows = hidden_by_z if c in Z_FIRST else hidden
-        value = dot(rows, down_w[:, :, cols].reshape(512, width)).astype(BF16)
-        moe_out[:, :, cols] = value.reshape(8, 16, width)
-        if c in Z_FIRST:
-            z_out(moe_out, ret1, 1, c)
-        else:
-            plane_back(moe_out, ret1, c)
-        if c == CHUNKS - 2:
-            second_hop(0)
-
-    for c in range(1, CHUNKS):
-        second_hop(c)
+            z_out(ret1p, ret2, 1, c, 9)
     for c in range(CHUNKS):
         cols = cols_of(c)
         phase(f"ret_2_{c}")
         if c in Z_FIRST:
-            plane_in(ret2, 1, c)
+            by_role(lambda blocks: ret2.at[blocks, :, cols], p_sem.at[1, c])
         else:
-            z_in(ret2, 1, c)
+            came(ret2.at[0:7, :, cols], z_sem.at[1, c])
         phase(f"combine_{c}")
         back = ret2[:, :, cols].reshape(128, width)
         order = 0 if c in Z_FIRST else 2
@@ -632,28 +654,26 @@
             left(mine2, plane_sem.at[0, d - 1])
 
     left(part.at[0:3], mix_sem.at[0])
-    for trip, (z_src, p_src) in enumerate(((disp, disp2), (ret1p, moe_out))):
-        left(z_src.at[0:7], hop_out_sem.at[trip, 0])
-
-        @pl.when(owner)
-        def _():
-            left(p_src.at[0:7], hop_out_sem.at[trip, 1])
-
-        @pl.when(guest)
-        def _():
-            left(p_src, hop_out_sem.at[trip, 1])
+    half = slice(0, 1024)
+    seven, eight = disp.at[0:7, :, half], disp.at[:, :, half]
+    for k in (0, 9):
+        left(seven, out_sem.at[k])
 
     @pl.when(owner)
     def _():
-        left(gate_up, part_out_sem.at[TO_SIBLING, 0])
-        left(down_w, part_out_sem.at[TO_SIBLING, 1])
-        left(gate_up.at[:, 0:2], part_out_sem.at[ACROSS, 0])
-        left(down_w.at[0:2], part_out_sem.at[ACROSS, 1])
+        for k in (1, 2, 3, 4, 6, 8):
+            left(seven, out_sem.at[k])
+        for k in (5, 7):
+            left(eight, out_sem.at[k])
+        left(gate_up.at[:, 0:2], part_out_sem.at[0])
+        left(down_w.at[0:2], part_out_sem.at[1])
 
     @pl.when(guest)
     def _():
-        left(gate_up.at[0, 0:2], part_out_sem.at[ACROSS, 0])
-        left(down_w.at[0], part_out_sem.at[ACROSS, 1])
+        for k in (1, 2, 3, 8):
+            left(eight, out_sem.at[k])
+        left(gate_up.at[0, 0:2], part_out_sem.at[0])
+        left(down_w.at[0], part_out_sem.at[1])
 
     phase()
 
@@ -714,20 +734,23 @@
             pltpu.VMEM((32, 2048), BF16),
             pltpu.VMEM((2, 128, 32), BF16),
             pltpu.VMEM((4, 32, 128), BF16),
-            wide, wide, wide, wide, wide, wide, wide, wide,
+            wide, wide, wide,
+            pltpu.VMEM((2, 8, 16, 2048), BF16),
+            pltpu.VMEM((2, 8, 16, 2048), BF16),
+            wide, wide, wide,
             pltpu.VMEM((32, 2048), F32),
             pltpu.SemaphoreType.DMA((len(operands),)),
             pltpu.SemaphoreType.DMA((3,)),
             pltpu.SemaphoreType.DMA((2,)),
             pltpu.SemaphoreType.DMA((3, 8)),
-            pltpu.SemaphoreType.DMA((5,)),
-            pltpu.SemaphoreType.DMA((2, 2)),
+            pltpu.SemaphoreType.DMA((2,)),
             pltpu.SemaphoreType.DMA((2,)),
             pltpu.SemaphoreType.DMA((2, 7)),
             pltpu.SemaphoreType.DMA((2,)),
             pltpu.SemaphoreType.DMA((2, CHUNKS)),
             pltpu.SemaphoreType.DMA((2, CHUNKS)),
-            pltpu.SemaphoreType.DMA((2, 2)),
+            pltpu.SemaphoreType.DMA((2, CHUNKS)),
+            pltpu.SemaphoreType.DMA((10,)),
         ],
         compiler_params=pltpu.CompilerParams(
             collective_id=0, has_side_effects=True, vmem_limit_bytes=56 * 2**20

time: 68 us -> 66.9 us (0.984)
  Pallas kernels: 66.3 us -> 65.2 us
    pallas_call x1, Pallas kernels: 66.3 us -> 65.2 us  [shards(): pl.pallas_call(mega, out_shape=jax.ShapeDtypeStruct((32, 2048), BF16), in...]
where the time goes in v6:
time: 66.9 us; the launch traced here: 66.8 us
  Pallas kernels  65.2 us (97%)
  local copies, waits for them, and re-layouts  1.57 us (2%)
    pallas_call x1, Pallas kernels, shards(): pl.pallas_call(mega, out_shape=jax.ShapeDtypeStruct((32, 2048), BF16), in...  65.2 us
    unnamed x1, local copies, waits for them, and re-layouts  1.57 us

profile of v6, /device:TPU:1, one launch (start us, length us, event | category | flops | bytes accessed | tf_op | source)
XLA Modules:
  0.0 66.8 jit_solution(5642526082927687772)
XLA Ops:
  0.0 65.2 %mega.1 = bf16[32,2048]{1,0:T(8,128)(2,1)} custom-call(bf16[32,2048]{1,0:T(8,128)(2,1)} %stream_h.1, bf16[128,2,256]{2,1,0:T(2,128)(2,1)} %rec_h.1, bf16[128,2,256]{2,1,0:T(2,128)(2,1)} %gatein_h.1, bf16[4,2,256]{2,1,0:T(2,128)(2,1)} %taps_h.1, bf16[2,4,64,64]{3,2,1,0:T(8,128)(2,1)} %small_gates_h.1, bf16[2,2,128,128]{3,2,1,0:T(8,128)(2,1)} %large_gates_h.1, ...), custom_call_target="tpu_custom_call" | custom-call | tf_op jit(solution)/shard_map/mega/pallas_call | solution.py:713
  65.2 1.6 %copy.23 = bf16[32,2048]{1,0:T(8,128)(2,1)} copy(bf16[32,2048]{1,0:T(8,128)(2,1)} %mega.1) | data formatting | bytes 262144

commit v7 on v6

--- a/solution.py
+++ b/solution.py
@@ -16,6 +16,15 @@
 TPS = 4
 HEAD_ROWS = 16
 CHUNKS = 4
+BACK = (
+    (slice(0, 512), "z"),
+    (slice(512, 1024), "z"),
+    (slice(1024, 1280), "z"),
+    (slice(1280, 1536), "plane"),
+    (slice(1536, 1792), "plane"),
+    (slice(1792, 2048), "plane"),
+)
+PIECES = 4 + len(BACK)
 FAR_FIRST = (4, 3, 5, 2, 6, 1, 7)
 
 
@@ -73,7 +82,7 @@
     part, mixed_buf, normed, slot_buf, weight_buf,
     disp, arr1, disp2, arr2, moe_out, ret1, ret1p, ret2, acc,
     load_sem, slot_sem, border_sem, part_sem, part_out_sem, carry_sem, plane_sem, mix_sem,
-    z_sem, p_sem, last_sem, out_sem,
+    first_sem, last_sem, back_sem, out_sem,
 ):
     sp = lax.axis_index("sp")
     tp = lax.axis_index("tp")
@@ -147,10 +156,10 @@
         (shared_gate_h, shared_gate), (shared_up_h, shared_up), (shared_down_h, shared_down),
         (gain2_h, gain2), (bias2_h, bias2),
     )
-    loads = []
-    for k, (src, dst) in enumerate(names):
-        loads.append(pltpu.make_async_copy(src, dst, load_sem.at[k]))
-        loads[-1].start()
+    loads = [pltpu.make_async_copy(src, dst, load_sem.at[k]) for k, (src, dst) in enumerate(names)]
+    urgent = (0, 7, 8)
+    for k in (*urgent, *(k for k in range(len(names)) if k not in urgent)):
+        loads[k].start()
     wholes = (gate_up.at[0], gate_up.at[1], down_w)
     owns = (own_gate, own_up, own_down)
     slot_loads = [
@@ -178,7 +187,7 @@
     def piece_of(ref, k, lead=()):
         if k < 4:
             return ref.at[(*lead, slice(1024 * (k % 2), 1024 * (k % 2) + 1024))]
-        return ref.at[(*lead, slice(None), slice(512 * (k - 4), 512 * (k - 4) + 512))]
+        return ref.at[(*lead, slice(None), BACK[k - 4][0])]
 
     def buffer_of(k):
         return k // 2 if k < 4 else 2
@@ -186,9 +195,12 @@
     def held_piece(k, at):
         return piece_of(wholes[buffer_of(k)], k, (at,))
 
+    def arrival(kind, k):
+        return part_sem.at[kind, k if kind == FROM_MIRROR else max(k - 3, 0)]
+
     def across(src, k, at, kind, tp_to, when):
         out = part_out_sem.at[int(k >= 4)]
-        send(src, held_piece(k, at), out, part_sem.at[kind, k], sp, tp_to, when=when)
+        send(src, held_piece(k, at), out, arrival(kind, k), sp, tp_to, when=when)
 
     def own_out(k):
         src = piece_of(owns[buffer_of(k)], k)
@@ -199,7 +211,7 @@
         across(src, k, tp, FROM_MIRROR, mirror, guest)
 
     def held(k, kind):
-        came(held_piece(k, origin[kind]), part_sem.at[kind, k])
+        came(held_piece(k, origin[kind]), arrival(kind, k))
 
     def relay(k):
         @pl.when(owner)
@@ -408,12 +420,11 @@
     def cols_of(c):
         return slice(width * c, width * c + width)
 
-    def z_out(src, dst, trip, c, out):
-        cols = cols_of(c)
+    def z_out(src, dst, cols, out, recv):
         for d in FAR_FIRST:
             to = (zi + d) % PLANES
             lands = dst.at[zi, :, cols]
-            send(src.at[to, :, cols], lands, out_sem.at[out], z_sem.at[trip, c], z_peer(d), tp)
+            send(src.at[to, :, cols], lands, out_sem.at[out], recv, z_peer(d), tp)
         dst[zi, :, cols] = src[zi, :, cols]
 
     def by_role(ref_of, sem):
@@ -433,7 +444,7 @@
                 expert = hosted + other * (1 - 2 * hosted)
                 if first:
                     core_to, lands = hosted, arr1.at[pi, :, cols]
-                    recv = p_sem.at[0, c]
+                    recv = first_sem.at[c]
                 else:
                     core_to, lands = expert, arr2.at[other, pi, :, cols]
                     recv = last_sem.at[other, c]
@@ -473,8 +484,7 @@
         def _():
             arr2[0, zi, :, cols] = src[zi, :, cols]
 
-    def expert_to_z(c):
-        cols = cols_of(c)
+    def expert_to_z(cols, recv):
         for d in (*FAR_FIRST, 0):
             to = (zi + d) % PLANES
             for group in (0, 1):
@@ -485,13 +495,12 @@
                     moe_out.at[group, to, :, cols],
                     ret1.at[zi, :, cols],
                     out_sem.at[4 + group],
-                    z_sem.at[1, c],
+                    recv,
                     to * PLANE + place + group * (1 - 2 * hosted),
                     tp,
                 ).start()
 
-    def expert_to_plane(c):
-        cols = cols_of(c)
+    def expert_to_plane(cols, recv):
         for d in (*FAR_FIRST, 0):
             j = (pi + d) % PLANE
             for group in (1, 0):
@@ -502,15 +511,14 @@
                     moe_out.at[group, j, :, cols],
                     ret1.at[place, :, cols],
                     out_sem.at[6 + group],
-                    p_sem.at[1, c],
+                    recv,
                     zi * PLANE + j,
                     mirror if group else tp,
                 ).start()
 
     home = jnp.where(owner, tp, mirror)
 
-    def plane_back(src, dst, c):
-        cols = cols_of(c)
+    def plane_back(src, dst, cols, recv):
         for dx in (2, 1, 3, 0):
             for target_core in (0, 1):
                 j = ((xi + dx) % 4) * 2 + target_core
@@ -518,7 +526,7 @@
                     src.at[j, :, cols],
                     dst.at[place, :, cols],
                     out_sem.at[8],
-                    p_sem.at[1, c],
+                    recv,
                     zi * PLANE + j,
                     home,
                     when=jnp.logical_or(guest, core != target_core) if dx == 0 else None,
@@ -531,9 +539,9 @@
     def permuted(rows):
         return dot(pick, rows).astype(BF16)
 
-    def swapped(src, c):
-        rows = src[:, :, cols_of(c)].reshape(128, width)
-        return dot(pick, rows).astype(BF16).reshape(8, 16, width)
+    def swapped(src, cols):
+        size = cols.stop - cols.start
+        return permuted(src[:, :, cols].reshape(128, size)).reshape(8, 16, size)
 
     Z_FIRST = tuple(range(CHUNKS // 2))
     P_FIRST = tuple(range(CHUNKS // 2, CHUNKS))
@@ -543,10 +551,10 @@
         value = dot(slot_buf[order], normed[:, cols]).astype(BF16)
         disp[:, :, cols] = value.reshape(8, 16, width)
         if c in Z_FIRST:
-            z_out(disp, arr1, 0, c, 0)
+            z_out(disp, arr1, cols, 0, first_sem.at[c])
         else:
             plane_out(disp, c, True)
-    for k in (4, 5, 6, 7):
+    for k in range(4, PIECES):
         own_mirror(k)
     phase("shared")
     for k in (16, 17, 18, 19, 20):
@@ -557,20 +565,20 @@
 
     for c in P_FIRST:
         phase(f"disp_p1_{c}")
-        by_role(lambda blocks: arr1.at[blocks, :, cols_of(c)], p_sem.at[0, c])
+        by_role(lambda blocks: arr1.at[blocks, :, cols_of(c)], first_sem.at[c])
         phase(f"disp_swap_{c}")
-        disp2[:, :, cols_of(c)] = swapped(arr1, c)
+        disp2[:, :, cols_of(c)] = swapped(arr1, cols_of(c))
         z_to_expert(disp2, c)
     for c in Z_FIRST:
         phase(f"disp_z1_{c}")
-        came(arr1.at[0:7, :, cols_of(c)], z_sem.at[0, c])
+        came(arr1.at[0:7, :, cols_of(c)], first_sem.at[c])
         phase(f"disp_swap_{c}")
-        disp2[:, :, cols_of(c)] = swapped(arr1, c)
+        disp2[:, :, cols_of(c)] = swapped(arr1, cols_of(c))
         plane_out(disp2, c, False)
         phase(f"relay_{c}")
-        for k in range(4 + 2 * c, 6 + 2 * c):
+        for k in range(4, 6) if c == 0 else range(6, PIECES):
             relay(k)
-            if k < 7:
+            if k + 1 < PIECES:
                 own_out(k + 1)
     phase()
 
@@ -580,8 +588,7 @@
         for copy in slot_loads:
             copy.wait()
         for kind in (FROM_MATE, FROM_FAR):
-            for k in (0, 1, 2, 3):
-                held(k, kind)
+            came(gate_up.at[:, origin[kind]], part_sem.at[kind, 0])
         both = None
         for c in [c for both_kinds in zip(Z_FIRST, P_FIRST) for c in both_kinds]:
             cols = cols_of(c)
@@ -604,41 +611,41 @@
         )
         by_plane = hidden
         by_z = jnp.concatenate([permuted(hidden[:128]), permuted(hidden[128:])], axis=0)
-        for c in range(CHUNKS):
-            cols = cols_of(c)
-            phase(f"down_arrive_{c}")
-            held(4 + c, FROM_MATE)
-            held(4 + c, FROM_FAR)
-            phase(f"down_{c}")
-            rows = by_z if c in Z_FIRST else by_plane
-            value = dot(rows, down_w[:, :, cols].reshape(512, width)).astype(BF16)
-            moe_out[:, :, :, cols] = value.reshape(2, 8, 16, width)
-            if c in Z_FIRST:
-                expert_to_z(c)
+        for n, (cols, way) in enumerate(BACK):
+            phase(f"down_arrive_{n}")
+            held(4 + n, FROM_MATE)
+            held(4 + n, FROM_FAR)
+            phase(f"down_{n}")
+            rows = by_z if way == "z" else by_plane
+            size = cols.stop - cols.start
+            value = dot(rows, down_w[:, :, cols].reshape(512, size)).astype(BF16)
+            moe_out[:, :, :, cols] = value.reshape(2, 8, 16, size)
+            if way == "z":
+                expert_to_z(cols, back_sem.at[0, n])
             else:
-                expert_to_plane(c)
+                expert_to_plane(cols, back_sem.at[0, n])
         phase()
 
-    for c in range(CHUNKS):
-        phase(f"ret_1_{c}")
-        sem = z_sem.at[1, c] if c in Z_FIRST else p_sem.at[1, c]
-        by_role(lambda blocks: ret1.at[blocks, :, cols_of(c)], sem)
-        phase(f"ret_swap_{c}")
-        ret1p[:, :, cols_of(c)] = swapped(ret1, c)
-        if c in Z_FIRST:
-            plane_back(ret1p, ret2, c)
+    for n in (0, 1, 3, 2, 4, 5):
+        cols, way = BACK[n]
+        phase(f"ret_1_{n}")
+        by_role(lambda blocks: ret1.at[blocks, :, cols], back_sem.at[0, n])
+        phase(f"ret_swap_{n}")
+        ret1p[:, :, cols] = swapped(ret1, cols)
+        if way == "z":
+            plane_back(ret1p, ret2, cols, back_sem.at[1, n])
         else:
-            z_out(ret1p, ret2, 1, c, 9)
-    for c in range(CHUNKS):
-        cols = cols_of(c)
-        phase(f"ret_2_{c}")
-        if c in Z_FIRST:
-            by_role(lambda blocks: ret2.at[blocks, :, cols], p_sem.at[1, c])
+            z_out(ret1p, ret2, cols, 9, back_sem.at[1, n])
+    for n in (0, 1, 3, 4, 2, 5):
+        cols, way = BACK[n]
+        phase(f"ret_2_{n}")
+        if way == "z":
+            by_role(lambda blocks: ret2.at[blocks, :, cols], back_sem.at[1, n])
         else:
-            came(ret2.at[0:7, :, cols], z_sem.at[1, c])
-        phase(f"combine_{c}")
-        back = ret2[:, :, cols].reshape(128, width)
-        order = 0 if c in Z_FIRST else 2
+            came(ret2.at[0:7, :, cols], back_sem.at[1, n])
+        phase(f"combine_{n}")
+        back = ret2[:, :, cols].reshape(128, cols.stop - cols.start)
+        order = 0 if way == "z" else 2
         acc[:, cols] = (
             acc[:, cols] + dot(weight_buf[order], back) + dot(weight_buf[order + 1], back)
         )
@@ -654,24 +661,28 @@
             left(mine2, plane_sem.at[0, d - 1])
 
     left(part.at[0:3], mix_sem.at[0])
-    half = slice(0, 1024)
-    seven, eight = disp.at[0:7, :, half], disp.at[:, :, half]
+    by_z_back = sum(cols.stop - cols.start for cols, way in BACK if way == "z")
+    sent_cols = {0: 1024, 1: 1024, 2: 1024, 3: 1024, 4: by_z_back, 5: by_z_back, 8: by_z_back}
+
+    def all_left(k, blocks):
+        left(disp.at[0:blocks, :, 0 : sent_cols.get(k, 2048 - by_z_back)], out_sem.at[k])
+
     for k in (0, 9):
-        left(seven, out_sem.at[k])
+        all_left(k, 7)
 
     @pl.when(owner)
     def _():
         for k in (1, 2, 3, 4, 6, 8):
-            left(seven, out_sem.at[k])
+            all_left(k, 7)
         for k in (5, 7):
-            left(eight, out_sem.at[k])
+            all_left(k, 8)
         left(gate_up.at[:, 0:2], part_out_sem.at[0])
         left(down_w.at[0:2], part_out_sem.at[1])
 
     @pl.when(guest)
     def _():
         for k in (1, 2, 3, 8):
-            left(eight, out_sem.at[k])
+            all_left(k, 8)
         left(gate_up.at[0, 0:2], part_out_sem.at[0])
         left(down_w.at[0], part_out_sem.at[1])
 
@@ -742,14 +753,14 @@
             pltpu.SemaphoreType.DMA((len(operands),)),
             pltpu.SemaphoreType.DMA((3,)),
             pltpu.SemaphoreType.DMA((2,)),
-            pltpu.SemaphoreType.DMA((3, 8)),
+            pltpu.SemaphoreType.DMA((3, PIECES)),
             pltpu.SemaphoreType.DMA((2,)),
             pltpu.SemaphoreType.DMA((2,)),
             pltpu.SemaphoreType.DMA((2, 7)),
             pltpu.SemaphoreType.DMA((2,)),
+            pltpu.SemaphoreType.DMA((CHUNKS,)),
             pltpu.SemaphoreType.DMA((2, CHUNKS)),
-            pltpu.SemaphoreType.DMA((2, CHUNKS)),
-            pltpu.SemaphoreType.DMA((2, CHUNKS)),
+            pltpu.SemaphoreType.DMA((2, len(BACK))),
             pltpu.SemaphoreType.DMA((10,)),
         ],
         compiler_params=pltpu.CompilerParams(

time: 66.9 us -> 65.6 us (0.981)
  Pallas kernels: 65.2 us -> 64 us
    pallas_call x1, Pallas kernels: 65.2 us -> 64 us  [shards(): pl.pallas_call(mega, out_shape=jax.ShapeDtypeStruct((32, 2048), BF16), in...]
where the time goes in v7:
time: 65.6 us; the launch traced here: 65.5 us
  Pallas kernels  64 us (98%)
  local copies, waits for them, and re-layouts  1.57 us (2%)
    pallas_call x1, Pallas kernels, shards(): pl.pallas_call(mega, out_shape=jax.ShapeDtypeStruct((32, 2048), BF16), in...  64 us
    unnamed x1, local copies, waits for them, and re-layouts  1.57 us

profile of v7, /device:TPU:1, one launch (start us, length us, event | category | flops | bytes accessed | tf_op | source)
XLA Modules:
  0.0 65.5 jit_solution(1667956639659149591)
XLA Ops:
  0.0 64.0 %mega.1 = bf16[32,2048]{1,0:T(8,128)(2,1)} custom-call(bf16[32,2048]{1,0:T(8,128)(2,1)} %stream_h.1, bf16[128,2,256]{2,1,0:T(2,128)(2,1)} %rec_h.1, bf16[128,2,256]{2,1,0:T(2,128)(2,1)} %gatein_h.1, bf16[4,2,256]{2,1,0:T(2,128)(2,1)} %taps_h.1, bf16[2,4,64,64]{3,2,1,0:T(8,128)(2,1)} %small_gates_h.1, bf16[2,2,128,128]{3,2,1,0:T(8,128)(2,1)} %large_gates_h.1, ...), custom_call_target="tpu_custom_call" | custom-call | tf_op jit(solution)/shard_map/mega/pallas_call | solution.py:724
  64.0 1.6 %copy.23 = bf16[32,2048]{1,0:T(8,128)(2,1)} copy(bf16[32,2048]{1,0:T(8,128)(2,1)} %mega.1) | data formatting | bytes 262144

commit v8 on v7

--- a/solution.py
+++ b/solution.py
@@ -545,7 +545,7 @@
 
     Z_FIRST = tuple(range(CHUNKS // 2))
     P_FIRST = tuple(range(CHUNKS // 2, CHUNKS))
-    for c in (*Z_FIRST, *P_FIRST):
+    for c in [c for pair_of in zip(Z_FIRST, P_FIRST) for c in pair_of]:
         cols = cols_of(c)
         order = int(c in P_FIRST)
         value = dot(slot_buf[order], normed[:, cols]).astype(BF16)
@@ -626,7 +626,7 @@
                 expert_to_plane(cols, back_sem.at[0, n])
         phase()
 
-    for n in (0, 1, 3, 2, 4, 5):
+    for n in (0, 1, 3, 4, 2, 5):
         cols, way = BACK[n]
         phase(f"ret_1_{n}")
         by_role(lambda blocks: ret1.at[blocks, :, cols], back_sem.at[0, n])

time: 65.6 us -> 65.5 us (level)
  no operation moved by 1% of the time
where the time goes in v8:
time: 65.5 us; the launch traced here: 65.4 us
  Pallas kernels  63.9 us (98%)
  local copies, waits for them, and re-layouts  1.57 us (2%)
    pallas_call x1, Pallas kernels, shards(): pl.pallas_call(mega, out_shape=jax.ShapeDtypeStruct((32, 2048), BF16), in...  63.9 us
    unnamed x1, local copies, waits for them, and re-layouts  1.57 us

profile of v8, /device:TPU:1, one launch (start us, length us, event | category | flops | bytes accessed | tf_op | source)
XLA Modules:
  0.0 65.4 jit_solution(7013892318296170033)
XLA Ops:
  0.0 63.9 %mega.1 = bf16[32,2048]{1,0:T(8,128)(2,1)} custom-call(bf16[32,2048]{1,0:T(8,128)(2,1)} %stream_h.1, bf16[128,2,256]{2,1,0:T(2,128)(2,1)} %rec_h.1, bf16[128,2,256]{2,1,0:T(2,128)(2,1)} %gatein_h.1, bf16[4,2,256]{2,1,0:T(2,128)(2,1)} %taps_h.1, bf16[2,4,64,64]{3,2,1,0:T(8,128)(2,1)} %small_gates_h.1, bf16[2,2,128,128]{3,2,1,0:T(8,128)(2,1)} %large_gates_h.1, ...), custom_call_target="tpu_custom_call" | custom-call | tf_op jit(solution)/shard_map/mega/pallas_call | solution.py:724
  63.9 1.6 %copy.23 = bf16[32,2048]{1,0:T(8,128)(2,1)} copy(bf16[32,2048]{1,0:T(8,128)(2,1)} %mega.1) | data formatting | bytes 262144
